TPU v7x, 128 devices: a whole 4x4x4 slice. The times are simulated.
128 devices in a mesh: ep: 32 (over z, y, core), tp: 4 (over x).
Axes of the slice: x: 4, y: 4, z: 4, core: 2. Of those that a mesh axis runs over, the one named last changes fastest.
Arguments:
- hidden_in: bfloat16 [1536, 2048], P('ep'), may hold values from -6 to 6
- carried_state: float32 [1536, 4, 128, 256], P('ep', 'tp'), may hold values from -6 to 6
- input_gain: bfloat16 [2048], replicated, may hold values from 0.099609375 to 1.8984375
- query_weight: bfloat16 [2048, 512], P(None, 'tp'), may hold values from -0.125 to 0.125
- key_weight: bfloat16 [2048, 512], P(None, 'tp'), may hold values from -0.125 to 0.125
- value_weight: bfloat16 [2048, 1024], P(None, 'tp'), may hold values from -0.125 to 0.125
- outgate_weight: bfloat16 [2048, 1024], P(None, 'tp'), may hold values from -0.125 to 0.125
- decay_weight: bfloat16 [2048, 512], P(None, 'tp'), may hold values from -0.5 to 0.5
- decay_shift: float32 [1536, 512], P('ep', 'tp'), may hold values from -0.7 to 0
- head_gain: bfloat16 [4, 256], P('tp'), may hold values from 0.099609375 to 1.8984375
- output_weight: bfloat16 [1024, 2048], P('tp'), may hold values from -0.1875 to 0.1875
- channel_gain: bfloat16 [2048], replicated, may hold values from 0.099609375 to 1.8984375
- branch_gate: bfloat16 [2048], replicated, may hold values from -0.125 to 0.125
- routes: int32 [1536, 2], P('ep'), may hold values from 0 to 31, all different within a row; in each aligned block of 48 rows (0 to 47, 48 to 95, ...) at most 5 rows name the same one
- route_weights: float32 [1536, 2], P('ep'), may hold values from 0.1 to 1
- expert_gate: bfloat16 [32, 2048, 3072], P('ep', None, 'tp'), may hold values from -0.125 to 0.125
- expert_up: bfloat16 [32, 2048, 3072], P('ep', None, 'tp'), may hold values from -0.125 to 0.125
- expert_down: bfloat16 [32, 3072, 2048], P('ep', 'tp'), may hold values from -0.109375 to 0.109375
- dense_gate: bfloat16 [2048, 4096], P('tp', 'ep'), may hold values from -0.125 to 0.125
- dense_up: bfloat16 [2048, 4096], P('tp', 'ep'), may hold values from -0.125 to 0.125
- dense_down: bfloat16 [4096, 2048], P('ep', 'tp'), may hold values from -0.09375 to 0.09375
Outputs:
- mixed: bfloat16 [1536, 2048], P('ep', 'tp')
- new_state: float32 [1536, 4, 128, 256], P('ep', 'tp')
Inputs may be any that keep to these rules, and one draw needn't show every extreme that they name: `routes`: each row names 2 different experts. Among the rows of one index of ep no expert is named more than 5 times, and in every draw some expert is named exactly 5 times by the rows of some index.
All inputs are finite; a program needn't handle non-finite values.
Results may differ from a plain program's by a relative error of at most 0.02.
Values may be sent and summed in bfloat16 or wider, within the bound.
A program may use at most 128 MiB of HBM per device.

v0:
```python
import jax
import jax.numpy as jnp
from jax import lax
from jax.sharding import PartitionSpec as P

EPSILON = 1e-06
TAU_DECAY = 16.0


def copy_for_each(shard, axis):
    devices = lax.axis_size(axis)
    return lax.all_to_all(
        jnp.broadcast_to(shard[None], (devices, *shard.shape)), axis, 0, 0, tiled=True
    )


def taken_together(shard, axis):
    return copy_for_each(shard, axis).astype(jnp.float32).sum(axis=0)


def cut_along(shard, dim, devices):
    before, after = (shard.shape[:dim], shard.shape[dim + 1 :])
    return jnp.moveaxis(shard.reshape(*before, devices, -1, *after), dim, 0)


def summed_on_arrival(shard, axis, dim):
    blocks = cut_along(shard, dim, lax.axis_size(axis))
    arrived = lax.all_to_all(blocks, axis, split_axis=0, concat_axis=0, tiled=True)
    return arrived.astype(jnp.float32).sum(axis=0)


def gather_turned(arrays, axis, dims):
    turned = [jnp.moveaxis(a, dim, 0) for a, dim in zip(arrays, dims)]
    both = jnp.concatenate([t.reshape(len(t), -1) for t in turned], axis=1)
    whole, at, finished = (lax.all_gather(both, axis, axis=0, tiled=True), 0, [])
    for t, dim in zip(turned, dims):
        section = whole[:, at : at + t[0].size].reshape(-1, *t.shape[1:])
        finished.append(jnp.moveaxis(section, 0, dim))
        at += t[0].size
    return tuple(finished)


def rms_factor(values):
    return lax.rsqrt(jnp.mean(values * values, axis=-1, keepdims=True) + EPSILON)


def rounded(values):
    return lax.optimization_barrier(values.astype(jnp.bfloat16)).astype(jnp.float32)


def matmul(left, right):
    return jnp.dot(left, right, preferred_element_type=jnp.float32)


def unit_totals(paired):
    return lax.psum(paired.astype(jnp.bfloat16), "tp").astype(jnp.float32)


def body(
    hidden_in,
    carried_state,
    input_gain,
    query_weight,
    key_weight,
    value_weight,
    outgate_weight,
    decay_weight,
    decay_shift,
    head_gain,
    output_weight,
    channel_gain,
    branch_gate,
    routes,
    route_weights,
    expert_gate,
    expert_up,
    expert_down,
    dense_gate,
    dense_up,
    dense_down,
):
    tokens_here, width = hidden_in.shape
    heads_here, key_dim, value_dim = carried_state.shape[1:]
    quarter = width // lax.axis_size("tp")
    lane_start = lax.axis_index("tp") * quarter
    inputs = hidden_in.astype(jnp.float32)
    normed = (inputs * rms_factor(inputs) * input_gain.astype(jnp.float32)).astype(jnp.bfloat16)
    query = matmul(normed, query_weight).astype(jnp.bfloat16)
    key_rows = matmul(normed, key_weight).astype(jnp.bfloat16)
    value_rows = matmul(normed, value_weight).astype(jnp.bfloat16)
    outgate = matmul(normed, outgate_weight).astype(jnp.bfloat16)
    decay = jnp.exp(jax.nn.log_sigmoid(matmul(normed, decay_weight)) / TAU_DECAY + decay_shift)
    decay = decay.reshape(tokens_here, heads_here, key_dim)
    query_scaled = query.astype(jnp.float32).reshape(
        tokens_here, heads_here, key_dim
    ) * key_dim ** (-0.5)
    key_vals = key_rows.astype(jnp.float32).reshape(tokens_here, heads_here, key_dim)
    value_vals = value_rows.astype(jnp.float32).reshape(tokens_here, heads_here, value_dim)
    new_state = decay[..., None] * carried_state + key_vals[..., None] * value_vals[:, :, None, :]
    readout = jnp.einsum("bhk,bhkv->bhv", query_scaled, new_state)
    gate_vals = jax.nn.silu(outgate.astype(jnp.float32).reshape(tokens_here, heads_here, value_dim))
    gated = (readout * rms_factor(readout) * head_gain.astype(jnp.float32) * gate_vals).astype(
        jnp.bfloat16
    )
    partial_out = rounded(matmul(gated.reshape(tokens_here, heads_here * value_dim), output_weight))
    attended = taken_together(partial_out.astype(jnp.bfloat16), "tp").astype(jnp.float32)
    middle = rounded(inputs + attended)
    scaled = middle * rms_factor(middle) * channel_gain.astype(jnp.float32)
    branch = jax.nn.sigmoid(jnp.sum(scaled * branch_gate.astype(jnp.float32), axis=-1))
    send_rows = scaled.astype(jnp.bfloat16)
    ffn_own = lax.dynamic_slice_in_dim(send_rows, lane_start, quarter, 1)
    middle_own = lax.dynamic_slice_in_dim(middle, lane_start, quarter, 1)
    expert_count = lax.axis_size("ep")
    topk = routes.shape[1]
    capacity = tokens_here * topk // expert_count + 2
    chosen = (
        routes[:, :, None] == jnp.arange(expert_count, dtype=jnp.int32)[None, None, :]
    ).astype(jnp.int32)
    chosen_flat = chosen.reshape(tokens_here * topk, expert_count)
    earlier = jnp.cumsum(chosen_flat, axis=0) - chosen_flat
    slot_index = jnp.sum(earlier * chosen_flat, axis=1).reshape(tokens_here, topk)
    position = routes * capacity + slot_index
    slot_table = jnp.arange(expert_count * capacity, dtype=jnp.int32)
    selector = jnp.sum(
        (slot_table[:, None, None] == position[None, :, :]).astype(jnp.bfloat16), axis=2
    )
    send_width = send_rows.shape[1]
    outgoing = (
        matmul(selector, send_rows).astype(jnp.bfloat16).reshape(expert_count, capacity, send_width)
    )
    received = lax.all_to_all(outgoing, "ep", split_axis=0, concat_axis=0, tiled=True)
    sources = received.shape[0]
    items = received.shape[1]
    flat_rows = received.reshape(sources * items, width)
    gate_part = matmul(flat_rows, expert_gate[0])
    up_part = matmul(flat_rows, expert_up[0])
    hidden = (jax.nn.silu(gate_part) * up_part).astype(jnp.bfloat16)
    block_out = rounded(matmul(hidden, expert_down[0]))
    summed = summed_on_arrival(block_out.astype(jnp.bfloat16), "tp", 1)
    returned = lax.all_to_all(
        summed.reshape(sources, items, quarter).astype(jnp.bfloat16),
        "ep",
        split_axis=0,
        concat_axis=0,
        tiled=True,
    ).astype(jnp.float32)
    flat_back = returned.reshape(expert_count * capacity, quarter)
    picked = jnp.take(flat_back, position.reshape(-1), axis=0).reshape(tokens_here, topk, quarter)
    routed_own = jnp.sum(picked * route_weights[:, :, None], axis=1)
    gate_all, up_all, down_all = gather_turned((dense_gate, dense_up, dense_down), "ep", (1, 1, 0))
    paired = unit_totals(
        jnp.concatenate([matmul(ffn_own, gate_all), matmul(ffn_own, up_all)], axis=1)
    )
    units = gate_all.shape[1]
    dense_hidden = (jax.nn.silu(paired[:, :units]) * paired[:, units:]).astype(jnp.bfloat16)
    dense_own = matmul(dense_hidden, down_all)
    mixed = (middle_own + branch[:, None] * dense_own + routed_own).astype(jnp.bfloat16)
    return (mixed, new_state)


def solution(mesh):
    in_specs = (
        P("ep", None),
        P("ep", "tp", None, None),
        P(),
        P(None, "tp"),
        P(None, "tp"),
        P(None, "tp"),
        P(None, "tp"),
        P(None, "tp"),
        P("ep", "tp"),
        P("tp", None),
        P("tp", None),
        P(),
        P(),
        P("ep", None),
        P("ep", None),
        P("ep", None, "tp"),
        P("ep", None, "tp"),
        P("ep", "tp", None),
        P("tp", "ep"),
        P("tp", "ep"),
        P("ep", "tp"),
    )
    out_specs = (P("ep", "tp"), P("ep", "tp", None, None))
    return jax.shard_map(body, mesh=mesh, in_specs=in_specs, out_specs=out_specs, check_vma=False)
```

profile of v0, /device:TPU:1, one launch (start us, length us, event | category | flops | bytes accessed | tf_op | source)
XLA Modules:
  0.0 166.0 jit_solution(2112288179264293746)
XLA Ops:
  7.2 0.0 all-gather.2.cloned.1.call-start
  7.2 1.2 copy.51
  8.4 1.7 %copy.50 = bf16[512,128]{0,1:T(8,128)(2,1)} copy(bf16[512,128]{1,0:T(8,128)(2,1)} %param.39) | data formatting | bytes 262144 | tf_op args[18]
  10.1 1.7 %pad_maximum_fusion.1 = bf16[128,1536]{1,0:T(8,128)(2,1)} fusion(bf16[128,512]{1,0:T(8,128)(2,1)} %param.41, bf16[128,512]{1,0:T(8,128)(2,1)S(1)} %bitcast.70, bf16[128,512]{1,0:T(8,128)(2,1)} %bitcast.71), kind=kLoop, calls=%fused_computation.52 | loop fusion | flops 1179648 | bytes 786432 | tf_op jit(solution)/shard_map/concatenate | solution.py:34
  11.8 0.0 all-gather.2.cloned.1.call-update
  11.9 0.7 convert_element_type.98
  12.6 0.7 mul.199
  13.2 1.1 fusion.46
  14.3 1.4 fusion.37
  15.7 1.4 fusion.35
  17.2 1.4 fusion.67
  18.6 1.6 fusion.34
  20.2 3.9 %fusion.84 = f32[48,1,256]{2,1,0:T(1,128)S(1)} fusion(f32[48,128,1]{1,2,0:T(1,128)S(1)} %bitcast.72, f32[48,256]{1,0:T(8,128)S(1)} %fusion.34, f32[48,128]{1,0:T(8,128)S(1)} %fusion.35, f32[48,1,128,256]{3,2,1,0:T(8,128)} %param.22, f32[48,128]{1,0:T(8,128)S(1)} %fusion.67), kind=kOutput, calls=%fused_computation.98 | convolution fusion | flops 7864320 | bytes 6463488 | tf_op jit(solution)/shard_map/bhk,bhkv->bhv/dot_general | solution.py:100
  24.1 0.1 fusion.56
  24.2 0.5 add_rsqrt_fusion.1
  24.7 2.5 %convolution_convert_fusion.3 = bf16[48,2048]{1,0:T(8,128)(2,1)S(1)} fusion(bf16[256,2048]{1,0:T(8,128)(2,1)} %param.31, bf16[2048,256]{1,0:T(8,128)(2,1)} %param.27, f32[48,1,256]{2,1,0:T(1,128)} %copy-done.3, f32[256]{0:T(256)S(1)} %bitcast.73, f32[48]{0:T(128)} %add_rsqrt_fusion.1, bf16[48,2048]{1,0:T(8,128)(2,1)S(1)} %copy-done.1, ...), kind=kOutput, calls=%fused_computation.18 | convolution fusion | flops 101277696 | bytes 2549120 | tf_op jit(solution)/shard_map/dot_general | solution.py:52
  27.2 1.0 broadcast_in_dim.9
  28.2 4.9 %all-to-all-start = ((bf16[4,48,2048]{2,1,0:T(8,128)(2,1)}), bf16[4,48,2048]{2,1,0:T(8,128)(2,1)}, u32[]{:S(2)}, u32[]{:S(2)}) async-start(bf16[4,48,2048]{2,1,0:T(8,128)(2,1)} %broadcast_in_dim.9), calls=%async_computation | async-start | bytes 1572864 | tf_op jit(solution)/shard_map/all_to_all | solution.py:12
  33.1 0.8 copy.52
  33.8 0.1 eq.29
  34.0 0.1 fusion.60
  34.0 0.1 reduce_window_sum.11
  34.2 0.2 select_reduce_fusion
  34.4 0.1 reshape.151
  34.5 0.1 copy.53
  34.6 0.7 convert_element_type.114
  35.3 0.7 convert_element_type.113
  36.0 1.2 compare_and_fusion
  37.1 0.7 fusion.55
  37.8 6.8 %all-to-all-done = bf16[4,48,2048]{2,1,0:T(8,128)(2,1)} async-done(((bf16[4,48,2048]{2,1,0:T(8,128)(2,1)}), bf16[4,48,2048]{2,1,0:T(8,128)(2,1)}, u32[]{:S(2)}, u32[]{:S(2)}) %all-to-all-start) | async-done | bytes 786464 | tf_op jit(solution)/shard_map/all_to_all | solution.py:12
  44.6 1.3 convert_reduce_fusion
  46.0 0.1 multiply_reduce_fusion.1
  46.1 0.8 multiply_reduce_fusion
  46.9 2.0 %convolution_convert_fusion.2 = bf16[160,2048]{1,0:T(8,128)(2,1)} fusion(bf16[160,48]{0,1:T(8,128)(2,1)} %fusion.55, bf16[48,2048]{1,0:T(8,128)(2,1)S(1)} %get-tuple-element.5), kind=kOutput, calls=%fused_computation.17 | convolution fusion | flops 31784960 | bytes 867328 | tf_op jit(solution)/shard_map/dot_general | solution.py:52
  48.9 2.2 %reshape.152 = bf16[32,5,2048]{2,1,0:T(8,128)(2,1)} reshape(bf16[160,2048]{1,0:T(8,128)(2,1)} %convolution_convert_fusion.2) | data formatting | bytes 1310720 | tf_op jit(solution)/shard_map/reshape | solution.py:129
  51.1 10.3 %all-to-all-start.1 = ((bf16[32,5,2048]{2,1,0:T(8,128)(2,1)}), bf16[32,5,2048]{2,1,0:T(8,128)(2,1)}, u32[]{:S(2)}, u32[]{:S(2)}) async-start(bf16[32,5,2048]{2,1,0:T(8,128)(2,1)} %reshape.152), calls=%async_computation.1 | async-start | bytes 2097152 | tf_op jit(solution)/shard_map/all_to_all | solution.py:131
  61.4 0.7 copy.56
  62.1 0.9 reshape.157
  63.0 0.1 copy.54
  63.1 1.4 copy.57
  64.5 23.4 %all-to-all-done.1 = bf16[32,5,2048]{2,1,0:T(8,128)(2,1)} async-done(((bf16[32,5,2048]{2,1,0:T(8,128)(2,1)}), bf16[32,5,2048]{2,1,0:T(8,128)(2,1)}, u32[]{:S(2)}, u32[]{:S(2)}) %all-to-all-start.1) | async-done | bytes 655392 | tf_op jit(solution)/shard_map/all_to_all | solution.py:131
  87.8 2.2 %reshape.153 = bf16[160,2048]{1,0:T(8,128)(2,1)} reshape(bf16[32,5,2048]{2,1,0:T(8,128)(2,1)} %all-to-all-done.1) | data formatting | bytes 1310720 | tf_op jit(solution)/shard_map/reshape | solution.py:134
  90.0 3.6 %fusion.10 = f32[160,768]{1,0:T(8,128)} fusion(bf16[160,2048]{1,0:T(8,128)(2,1)} %reshape.153, bf16[1,2048,768]{2,1,0:T(8,128)(2,1)} %param.36), kind=kOutput, calls=%fused_computation.14 | convolution fusion | flops 503316480 | bytes 4292608 | tf_op jit(solution)/shard_map/dot_general | solution.py:52
  93.6 4.5 %fusion.12 = bf16[160,2048]{1,0:T(8,128)(2,1)} fusion(bf16[1,768,2048]{2,1,0:T(8,128)(2,1)S(1)} %copy-done, bf16[160,2048]{1,0:T(8,128)(2,1)} %reshape.153, bf16[1,2048,768]{2,1,0:T(8,128)(2,1)} %param.37, f32[160,768]{1,0:T(8,128)} %fusion.10), kind=kOutput, calls=%fused_computation.16 | convolution fusion | flops 1007697920 | bytes 8093696 | tf_op jit(solution)/shard_map/dot_general | solution.py:52
  98.1 2.0 %copy.67 = bf16[20,4,8,512]{3,2,0,1:T(8,128)(2,1)} copy(bf16[20,4,8,512]{3,2,1,0:T(8,128)(2,1)} %bitcast.69) | data formatting | bytes 1310720 | tf_op jit(solution)/shard_map/reshape | solution.py:23
  100.1 4.2 %all-to-all-start.2 = ((bf16[4,160,512]{2,1,0:T(8,128)(2,1)}), bf16[4,160,512]{2,1,0:T(8,128)(2,1)}, u32[]{:S(2)}, u32[]{:S(2)}) async-start(bf16[4,160,512]{2,1,0:T(8,128)(2,1)} %bitcast.68), calls=%async_computation.2 | async-start | bytes 1310720 | tf_op jit(solution)/shard_map/all_to_all | solution.py:28
  104.2 0.0 all-reduce.2.cloned.1.call-start
  104.3 0.0 all-gather.2.cloned.1.call-done
  104.3 3.5 %convolution_convert_fusion = bf16[48,4096]{1,0:T(8,128)(2,1)S(1)} fusion(bf16[4096,1536]{1,0:T(8,128)(2,1)} %all-gather.2.cloned.1.call-done, bf16[48,2048]{1,0:T(8,128)(2,1)S(1)} %get-tuple-element.5, s32[]{:T(128)S(6)} %select_n.32), kind=kOutput, calls=%fused_computation.4 | convolution fusion | flops 201523200 | bytes 4636676 | tf_op jit(solution)/shard_map/dot_general | solution.py:52
  107.9 3.5 %convolution_convert_fusion.1 = bf16[48,4096]{1,0:T(8,128)(2,1)S(1)} fusion(bf16[4096,1536]{1,0:T(8,128)(2,1)} %all-gather.2.cloned.1.call-done, bf16[48,2048]{1,0:T(8,128)(2,1)S(1)} %get-tuple-element.5, s32[]{:T(128)S(6)} %select_n.32), kind=kOutput, calls=%fused_computation.5 | convolution fusion | flops 201523200 | bytes 4636676 | tf_op jit(solution)/shard_map/dot_general | solution.py:52
  111.4 0.9 pad_maximum_fusion
  112.4 7.3 %multiply_add_fusion = f32[48,1,128,256]{3,2,1,0:T(8,128)} fusion(f32[48,1,128,256]{3,2,1,0:T(8,128)} %param.22, f32[48,256]{1,0:T(8,128)} %copy-done.2, f32[48,128]{1,0:T(8,128)} %copy-done.4, f32[48,128]{1,0:T(8,128)} %copy-done.5), kind=kLoop, calls=%fused_computation.3 | loop fusion | flops 4718592 | bytes 12681216 | tf_op jit(solution)/shard_map/add | solution.py:99
  119.7 0.8 convert_element_type.112
  120.4 1.2 reduce_sum.94
  121.7 0.8 convert_element_type.123
  122.4 6.7 %all-to-all-start.3 = ((bf16[32,5,512]{2,1,0:T(8,128)(2,1)}), bf16[32,5,512]{2,1,0:T(8,128)(2,1)}, u32[]{:S(2)}, u32[]{:S(2)}) async-start(bf16[32,5,512]{2,1,0:T(8,128)(2,1)} %convert_element_type.123), calls=%async_computation.3 | async-start | bytes 524288 | tf_op jit(solution)/shard_map/all_to_all | solution.py:140
  129.2 9.0 %all-to-all-done.3 = bf16[32,5,512]{2,1,0:T(8,128)(2,1)} async-done(((bf16[32,5,512]{2,1,0:T(8,128)(2,1)}), bf16[32,5,512]{2,1,0:T(8,128)(2,1)}, u32[]{:S(2)}, u32[]{:S(2)}) %all-to-all-start.3) | async-done | bytes 163872 | tf_op jit(solution)/shard_map/all_to_all | solution.py:140
  138.2 1.0 reshape.160
  139.2 1.4 gather_fusion
  140.6 1.0 gather.7
  141.7 0.3 multiply_reduce_fusion.2
  142.0 12.3 %all-reduce.2.cloned.1.call-done = bf16[48,8192]{1,0:T(8,128)(2,1)} async-done(((bf16[48,8192]{1,0:T(8,128)(2,1)}), bf16[48,8192]{1,0:T(8,128)(2,1)}) %all-reduce.2.cloned.1.call-update) | async-done | bytes 786448 | tf_op jit(solution)/shard_map/psum | solution.py:56
  154.3 1.2 convert_element_type.116
  155.6 3.6 %fusion.30 = bf16[48,512]{1,0:T(8,128)(2,1)} fusion(f32[48,512]{1,0:T(8,128)S(1)} %multiply_reduce_fusion.2, bf16[4096,1536]{1,0:T(8,128)(2,1)} %all-gather.2.cloned.1.call-done, f32[48,8192]{1,0:T(8,128)S(1)} %convert_element_type.116, f32[48,2048]{1,0:T(8,128)} %convert_element_type.112, s32[]{:T(128)S(6)} %select_n.32, f32[48]{0:T(128)S(1)} %add_divide_fusion), kind=kOutput, calls=%fused_computation.25 | convolution fusion | flops 202604544 | bytes 6013124 | tf_op jit(solution)/shard_map/dot_general | solution.py:52
  (30 shorter events, 0.1 us)
Async XLA Ops:
  7.2 86.4 %copy-start = (bf16[1,768,2048]{2,1,0:T(8,128)(2,1)S(1)}, bf16[1,768,2048]{2,1,0:T(8,128)(2,1)}, u32[]{:S(2)}) copy-start(bf16[1,768,2048]{2,1,0:T(8,128)(2,1)} %param.38) | copy-start | bytes 9437188
  7.2 11.4 %copy-start.1 = (bf16[48,2048]{1,0:T(8,128)(2,1)S(1)}, bf16[48,2048]{1,0:T(8,128)(2,1)}, u32[]{:S(2)}) copy-start(bf16[48,2048]{1,0:T(8,128)(2,1)} %param.21) | copy-start | bytes 589828
  7.2 97.1 %all-gather.2.cloned.1.call-start = ((), (), s32[]{:S(2)}) async-start(), calls=%async_computation.4 | async-start | bytes 12976128 | tf_op jit(solution)/shard_map/all_gather | solution.py:35
  17.2 6.9 %copy-start.4 = (f32[48,128]{1,0:T(8,128)}, f32[48,128]{1,0:T(8,128)S(1)}, u32[]{:S(2)}) copy-start(f32[48,128]{1,0:T(8,128)S(1)} %fusion.35) | copy-start | bytes 73732
  18.6 6.2 %copy-start.5 = (f32[48,128]{1,0:T(8,128)}, f32[48,128]{1,0:T(8,128)S(1)}, u32[]{:S(2)}) copy-start(f32[48,128]{1,0:T(8,128)S(1)} %fusion.67) | copy-start | bytes 73732
  20.2 4.6 %copy-start.2 = (f32[48,256]{1,0:T(8,128)}, f32[48,256]{1,0:T(8,128)S(1)}, u32[]{:S(2)}) copy-start(f32[48,256]{1,0:T(8,128)S(1)} %fusion.34) | copy-start | bytes 147460
  24.1 0.7 copy-start.3
  28.2 16.4 %all-to-all-start = ((bf16[4,48,2048]{2,1,0:T(8,128)(2,1)}), bf16[4,48,2048]{2,1,0:T(8,128)(2,1)}, u32[]{:S(2)}, u32[]{:S(2)}) async-start(bf16[4,48,2048]{2,1,0:T(8,128)(2,1)} %broadcast_in_dim.9), calls=%async_computation | async-start | bytes 1572864 | tf_op jit(solution)/shard_map/all_to_all | solution.py:12
  37.1 7.5 %copy-start.7 = (s32[48,2]{0,1:T(2,128)}, s32[48,2]{0,1:T(2,128)S(1)}, u32[]{:S(2)}) copy-start(s32[48,2]{0,1:T(2,128)S(1)} %get-tuple-element.3) | copy-start | bytes 1156
  46.9 14.5 %copy-start.8 = (s32[48,2]{0,1:T(2,128)S(1)}, s32[48,2]{0,1:T(2,128)}, u32[]{:S(2)}) copy-start(s32[48,2]{0,1:T(2,128)} %copy-done.7) | copy-start | bytes 1156
  46.9 16.1 %copy-start.9 = (pred[48,2]{0,1:T(4,128)(4,1)S(1)}, pred[48,2]{0,1:T(4,128)(4,1)}, u32[]{:S(2)}) copy-start(pred[48,2]{0,1:T(4,128)(4,1)} %get-tuple-element.2) | copy-start | bytes 292
  51.1 36.8 %all-to-all-start.1 = ((bf16[32,5,2048]{2,1,0:T(8,128)(2,1)}), bf16[32,5,2048]{2,1,0:T(8,128)(2,1)}, u32[]{:S(2)}, u32[]{:S(2)}) async-start(bf16[32,5,2048]{2,1,0:T(8,128)(2,1)} %reshape.152), calls=%async_computation.1 | async-start | bytes 2097152 | tf_op jit(solution)/shard_map/all_to_all | solution.py:131
  100.1 20.4 %all-to-all-start.2 = ((bf16[4,160,512]{2,1,0:T(8,128)(2,1)}), bf16[4,160,512]{2,1,0:T(8,128)(2,1)}, u32[]{:S(2)}, u32[]{:S(2)}) async-start(bf16[4,160,512]{2,1,0:T(8,128)(2,1)} %bitcast.68), calls=%async_computation.2 | async-start | bytes 1310720 | tf_op jit(solution)/shard_map/all_to_all | solution.py:28
  104.2 50.1 %all-reduce.2.cloned.1.call-start = ((), (), s32[]{:S(2)}) async-start(), calls=%async_computation.5 | async-start | bytes 1572864 | tf_op jit(solution)/shard_map/psum | solution.py:56
  112.3 16.8 %copy-start.10 = (f32[48]{0:T(128)S(1)}, f32[48]{0:T(128)}, u32[]{:S(2)}) copy-start(f32[48]{0:T(128)} %get-tuple-element.4) | copy-start | bytes 580
  120.4 21.2 %copy-start.6 = (f32[48,2]{1,0:T(8,128)S(1)}, f32[48,2]{1,0:T(8,128)}, u32[]{:S(2)}) copy-start(f32[48,2]{1,0:T(8,128)} %copy.57) | copy-start | bytes 1156
  122.4 15.8 %all-to-all-start.3 = ((bf16[32,5,512]{2,1,0:T(8,128)(2,1)}), bf16[32,5,512]{2,1,0:T(8,128)(2,1)}, u32[]{:S(2)}, u32[]{:S(2)}) async-start(bf16[32,5,512]{2,1,0:T(8,128)(2,1)} %convert_element_type.123), calls=%async_computation.3 | async-start | bytes 524288 | tf_op jit(solution)/shard_map/all_to_all | solution.py:140
Sparse Core Ops, SparseCore 0:
  12.0 77.4 all-gather.1
  112.5 41.8 all-reduce.1
where the time goes:
time: 169 us; the launch traced here: 166 us
  waiting for transfers between devices  51.5 us (30%)
  matrix products  32.9 us (19%)
  starting transfers between devices  26.2 us (16%)
  other arithmetic  22.6 us (13%)
  local copies, waits for them, and re-layouts  18.5 us (11%)
  between operations  14.3 us (8%)
    dot_general x11, matrix products, matmul(): return jnp.dot(left, right, preferred_element_type=jnp.float32)  29 us
    all_to_all x1, waiting for transfers between devices, body(): lax.all_to_all(outgoing, 'ep', split_axis=0, concat_axis=0, tiled=True)  23.4 us
    psum x1, waiting for transfers between devices, unit_totals(): return lax.psum(paired.astype(jnp.bfloat16), 'tp').astype(jnp.float32)  12.3 us
    all_to_all x1, starting transfers between devices, body(): lax.all_to_all(outgoing, 'ep', split_axis=0, concat_axis=0, tiled=True)  10.3 us
    all_to_all x1, waiting for transfers between devices, body(): lax.all_to_all(summed.reshape(sources, items, quarter).astype(jnp.bfloat1...  9.01 us
    add x1, other arithmetic, body(): decay[..., None] * carried_state  7.31 us
    all_to_all x1, waiting for transfers between devices, copy_for_each(): lax.all_to_all(jnp.broadcast_to(shard[None], (devices, *shard.shape)), ax...  6.79 us
    all_to_all x1, starting transfers between devices, body(): lax.all_to_all(summed.reshape(sources, items, quarter).astype(jnp.bfloat1...  6.74 us
  transfers between devices with their start and end apart: 6, of which 4 were waited for; matrix products, arithmetic and copies ran while one was open for 39% of the time, Pallas kernels for 0%

commit v1 on v0

v1 whole, which is shorter than its diff:
```python
import functools

import jax
import jax.numpy as jnp
from jax import lax
from jax.experimental import pallas as pl
from jax.experimental.pallas import tpu as pltpu
from jax.sharding import PartitionSpec as P

EPSILON = 1e-06
TAU_DECAY = 16.0
MESH = pl.DeviceIdType.MESH
CAP = 5
ROWS = 6
PAD = 8
Z_SIZE = 4
F32 = jnp.float32
BF16 = jnp.bfloat16


def dot(left, right):
    return jnp.dot(left, right, preferred_element_type=F32)


def rms_factor(values):
    return lax.rsqrt(jnp.mean(values * values, axis=-1, keepdims=True) + EPSILON)


def silu(values):
    return values * jax.nn.sigmoid(values)


def attention_kernel(
    experts,
    hid_ref,
    gain_ref,
    shift_ref,
    hgain_ref,
    routes_ref,
    rw_ref,
    qw_hbm,
    kw_hbm,
    vw_hbm,
    ow_hbm,
    dw_hbm,
    pw_hbm,
    state_hbm,
    part_ref,
    state_out,
    sel_ref,
    comb_hi_ref,
    comb_lo_ref,
    qw,
    kw,
    vw,
    ow,
    dw,
    pw,
    st,
    q_s,
    k_s,
    v_s,
    d_s,
    ro_s,
    w_sem,
    in_sem,
    out_sem,
):
    tokens, key_dim = q_s.shape
    groups = tokens // 8
    pairs = ((dw_hbm, dw), (qw_hbm, qw), (kw_hbm, kw), (vw_hbm, vw))
    w_copies = [pltpu.make_async_copy(s, d, w_sem.at[i]) for i, (s, d) in enumerate(pairs)]
    for copy in w_copies:
        copy.start()

    def state_in(g):
        rows = pl.ds(g * 8, 8)
        return pltpu.make_async_copy(state_hbm.at[rows], st.at[rows], in_sem.at[g])

    def state_back(g):
        rows = pl.ds(g * 8, 8)
        return pltpu.make_async_copy(st.at[rows], state_out.at[rows], out_sem.at[g])

    for g in range(groups):
        state_in(g).start()
    o_copy = pltpu.make_async_copy(ow_hbm, ow, w_sem.at[4])
    o_copy.start()
    p_copy = pltpu.make_async_copy(pw_hbm, pw, w_sem.at[5])
    p_copy.start()

    slots = experts * PAD
    e_at = lax.broadcasted_iota(jnp.int32, (tokens, experts), 1)
    r0, r1 = routes_ref[:, 0:1], routes_ref[:, 1:2]
    oh0, oh1 = (e_at == r0).astype(F32), (e_at == r1).astype(F32)
    tri = (
        lax.broadcasted_iota(jnp.int32, (tokens, tokens), 0)
        > lax.broadcasted_iota(jnp.int32, (tokens, tokens), 1)
    ).astype(F32)
    before0 = dot(tri, oh0)
    before1 = dot(tri, oh1) + jnp.sum(oh0, axis=0, keepdims=True)
    slot0 = jnp.sum(before0 * oh0, axis=1, keepdims=True)
    slot1 = jnp.sum(before1 * oh1, axis=1, keepdims=True)
    pos0 = r0 * PAD + slot0.astype(jnp.int32)
    pos1 = r1 * PAD + slot1.astype(jnp.int32)
    at = lax.broadcasted_iota(jnp.int32, (tokens, slots), 1)
    hit0, hit1 = (at == pos0).astype(F32), (at == pos1).astype(F32)
    sel_ref[...] = (hit0 + hit1).astype(BF16)
    comb = hit0 * rw_ref[:, 0:1] + hit1 * rw_ref[:, 1:2]
    comb_hi = comb.astype(BF16)
    comb_hi_ref[...] = comb_hi
    comb_lo_ref[...] = (comb - comb_hi.astype(F32)).astype(BF16)

    hid = hid_ref[...].astype(F32)
    normed = (hid * rms_factor(hid) * gain_ref[...].astype(F32)).astype(BF16)
    w_copies[0].wait()
    pre = dot(normed, dw[...])
    log_sig = jnp.minimum(pre, 0.0) - jnp.log1p(jnp.exp(-jnp.abs(pre)))
    d_s[...] = jnp.exp(log_sig / TAU_DECAY + shift_ref[...])
    w_copies[1].wait()
    q_s[...] = dot(normed, qw[...]).astype(BF16).astype(F32) * key_dim ** (-0.5)
    w_copies[2].wait()
    k_s[...] = dot(normed, kw[...]).astype(BF16).astype(F32)
    w_copies[3].wait()
    v_s[...] = dot(normed, vw[...]).astype(BF16).astype(F32)

    def group(g, carry):
        state_in(g).wait()
        rows = pl.ds(pl.multiple_of(g * 8, 8), 8)
        d_t, k_t, q_t = d_s[rows, :].T, k_s[rows, :].T, q_s[rows, :].T
        v_8 = v_s[rows, :]
        outs = []
        for j in range(8):
            new = d_t[:, j : j + 1] * st[g * 8 + j] + k_t[:, j : j + 1] * v_8[j : j + 1, :]
            st[g * 8 + j] = new
            outs.append(jnp.sum(q_t[:, j : j + 1] * new, axis=0, keepdims=True))
        ro_s[rows, :] = jnp.concatenate(outs, axis=0)

        @pl.when(g > 0)
        def _():
            state_back(g - 1).start()

        return carry

    lax.fori_loop(0, groups, group, 0)

    o_copy.wait()
    outgate = dot(normed, ow[...]).astype(BF16).astype(F32)
    readout = ro_s[...]
    gated = readout * rms_factor(readout) * hgain_ref[...].astype(F32) * silu(outgate)
    state_back(groups - 1).start()
    p_copy.wait()
    part_ref[...] = dot(gated.astype(BF16), pw[...]).astype(BF16)
    for g in range(groups):
        state_back(g).wait()


def attention(experts, hid, gain, shift, hgain, routes, rw, weights, pw, state):
    tokens, width = hid.shape
    key_dim, value_dim = state.shape[1:]
    slots = experts * PAD
    vmem = pl.BlockSpec(memory_space=pltpu.VMEM)
    anyspace = pl.BlockSpec(memory_space=pltpu.HBM)
    groups = tokens // 8
    return pl.pallas_call(
        functools.partial(attention_kernel, experts),
        name="attention",
        out_shape=(
            jax.ShapeDtypeStruct((tokens, width), BF16),
            jax.ShapeDtypeStruct(state.shape, F32),
            jax.ShapeDtypeStruct((tokens, slots), BF16),
            jax.ShapeDtypeStruct((tokens, slots), BF16),
            jax.ShapeDtypeStruct((tokens, slots), BF16),
        ),
        in_specs=[vmem] * 6 + [anyspace] * 7,
        out_specs=(vmem, anyspace, vmem, vmem, vmem),
        scratch_shapes=[pltpu.VMEM(w.shape, BF16) for w in weights]
        + [
            pltpu.VMEM(pw.shape, BF16),
            pltpu.VMEM(state.shape, F32),
            pltpu.VMEM((tokens, key_dim), F32),
            pltpu.VMEM((tokens, key_dim), F32),
            pltpu.VMEM((tokens, value_dim), F32),
            pltpu.VMEM((tokens, key_dim), F32),
            pltpu.VMEM((tokens, value_dim), F32),
            pltpu.SemaphoreType.DMA((6,)),
            pltpu.SemaphoreType.DMA((groups,)),
            pltpu.SemaphoreType.DMA((groups,)),
        ],
        compiler_params=pltpu.CompilerParams(vmem_limit_bytes=40 << 20),
    )(hid, gain, shift, hgain, routes, rw, *weights, pw, state)


def branches_kernel(
    sizes,
    part_ref,
    hid_ref,
    gain_ref,
    bgate_ref,
    sel_ref,
    comb_hi_ref,
    comb_lo_ref,
    eg_hbm,
    eu_hbm,
    ed_hbm,
    dg_hbm,
    du_hbm,
    dd_hbm,
    out_ref,
    eg,
    eu,
    ed,
    wgu,
    wd,
    rs1,
    mid,
    snd,
    rcv,
    ffn_all,
    pr,
    rs2,
    hid_all,
    db,
    dr,
    hbuf,
    yb,
    yr,
    rb,
    ret,
    local_sem,
    wz_send,
    wz_recv,
    x_send,
    x_recv,
    yc_send,
    yc_recv,
    pl_send,
    pl_recv,
):
    n_ep, n_x, n_z = sizes
    n_yc = n_ep // n_z
    tokens, width = hid_ref.shape
    quarter = width // n_x
    units = dg_hbm.shape[1]
    all_units = n_z * units
    ep, x = lax.axis_index("ep"), lax.axis_index("tp")
    z, yc = ep // n_yc, ep % n_yc

    def x_peer(i):
        return (ep, lax.rem(x + i, n_x))

    def z_peer(i):
        return (lax.rem(z + i, n_z) * n_yc + yc, x)

    def yc_peer(i):
        return (z * n_yc + lax.rem(yc + i, n_yc), x)

    def ep_peer(i):
        return (lax.rem(ep + i, n_ep), x)

    def remote(src, dst, send, recv, device):
        return pltpu.make_async_remote_copy(
            src_ref=src,
            dst_ref=dst,
            send_sem=send,
            recv_sem=recv,
            device_id=device,
            device_id_type=MESH,
        )

    e_copies = [
        pltpu.make_async_copy(s, d, local_sem.at[i])
        for i, (s, d) in enumerate(((eg_hbm, eg), (eu_hbm, eu), (ed_hbm, ed)))
    ]

    def unit_block(offset):
        return pl.ds(pl.multiple_of(offset + z * units, units), units)

    places = (
        (dg_hbm, wgu.at[:, unit_block(0)]),
        (du_hbm, wgu.at[:, unit_block(all_units)]),
        (dd_hbm, wd.at[unit_block(0), :]),
    )
    d_copies = [
        pltpu.make_async_copy(s, d, local_sem.at[3 + i]) for i, (s, d) in enumerate(places)
    ]

    rcv[...] = jnp.zeros_like(rcv)
    ret[...] = jnp.zeros_like(ret)

    barrier = pltpu.get_barrier_semaphore()
    for i in range(1, n_x):
        pl.semaphore_signal(barrier, inc=1, device_id=x_peer(i), device_id_type=MESH)

    def greet(i, carry):
        pl.semaphore_signal(barrier, inc=1, device_id=ep_peer(i), device_id_type=MESH)
        return carry

    lax.fori_loop(1, n_ep, greet, 0)
    for copy in d_copies + e_copies:
        copy.start()
    pl.semaphore_wait(barrier, n_x - 1 + n_ep - 1)

    def lanes(i):
        return pl.ds(pl.multiple_of(lax.rem(x + i, n_x) * quarter, quarter), quarter)

    rs1_copies = [
        remote(part_ref.at[:, lanes(i)], rs1.at[i], x_send.at[0, i], x_recv.at[0, i], x_peer(i))
        for i in range(1, n_x)
    ]
    for copy in rs1_copies:
        copy.start()
    wz_copies = [
        remote(s, d, wz_send.at[i, k], wz_recv.at[i, k], z_peer(i))
        for i in range(1, n_z)
        for k, (s, d) in enumerate(places)
    ]
    for copy in wz_copies:
        copy.start()
    total = part_ref[:, lanes(0)].astype(F32)
    for i, copy in zip(range(1, n_x), rs1_copies):
        copy.wait_recv()
        total = total + rs1[i].astype(F32)
    middle_q = (hid_ref[:, lanes(0)].astype(F32) + total).astype(BF16)
    mid[pl.ds(x, 1)] = middle_q[None]

    mid_copies = [
        remote(mid.at[x], mid.at[x], x_send.at[1, i], x_recv.at[1, i], x_peer(i))
        for i in range(1, n_x)
    ]
    for copy in mid_copies:
        copy.start()
    for copy in mid_copies:
        copy.wait_recv()
    squares = sum(
        jnp.sum(mid[i].astype(F32) * mid[i].astype(F32), axis=-1, keepdims=True) for i in range(n_x)
    )
    factor = lax.rsqrt(squares / width + EPSILON)
    own_scaled = mid[pl.ds(x, 1)][0].astype(F32) * factor * gain_ref[:, lanes(0)].astype(F32)
    ffn_all[pl.ds(yc, 1)] = own_scaled.astype(BF16)[None]
    yc_copies = [
        remote(
            ffn_all.at[yc], ffn_all.at[yc], yc_send.at[0, i], yc_recv.at[0, i], yc_peer(i)
        )
        for i in range(1, n_yc)
    ]
    for copy in yc_copies:
        copy.start()
    logit = jnp.zeros((tokens, 1), F32)
    for i in range(n_x):
        part = slice(i * quarter, (i + 1) * quarter)
        scaled = mid[i].astype(F32) * factor * gain_ref[:, part].astype(F32)
        logit = logit + jnp.sum(scaled * bgate_ref[:, part].astype(F32), axis=-1, keepdims=True)
        rows = lax.dot_general(
            sel_ref[...], scaled.astype(BF16), (((0,), (0,)), ((), ())), preferred_element_type=F32
        )
        snd[:, :, part] = rows.reshape(n_ep, PAD, quarter).astype(BF16)
    branch = jax.nn.sigmoid(logit)

    def dispatch(i, carry):
        to = lax.rem(ep + i, n_ep)
        remote(
            snd.at[to, pl.ds(0, ROWS)],
            rcv.at[ep, pl.ds(0, ROWS)],
            pl_send.at[0],
            pl_recv.at[0],
            (to, x),
        ).start()
        return carry

    lax.fori_loop(1, n_ep, dispatch, 0)
    rcv[pl.ds(ep, 1)] = snd[pl.ds(ep, 1)]

    for copy in d_copies:
        copy.wait()
    for copy in wz_copies:
        copy.wait_recv()
    for copy in yc_copies:
        copy.wait_recv()
    per_x = n_yc // n_x

    def paired_of(i):
        mine = ffn_all[pl.ds(lax.rem(x + i, n_x) * per_x, per_x)]
        return dot(mine.reshape(per_x * tokens, quarter), wgu[...])

    rs2_copies = []
    for i in range(1, n_x):
        pr[i] = paired_of(i).astype(BF16)
        rs2_copies.append(
            remote(pr.at[i], rs2.at[i], x_send.at[2, i], x_recv.at[2, i], x_peer(i))
        )
        rs2_copies[-1].start()
    paired = paired_of(0)

    for copy in e_copies:
        copy.wait()
    arrived = rcv.at[pl.ds(0, n_ep - 1), pl.ds(0, ROWS)]
    pltpu.make_async_copy(arrived, arrived, pl_recv.at[0]).wait()
    flat = n_ep * PAD
    tile = 256

    def hidden_tile(j, carry):
        cols = pl.ds(pl.multiple_of(j * tile, tile), tile)
        rows = rcv[...].reshape(flat, width)
        gate, up = dot(rows, eg[:, cols]), dot(rows, eu[:, cols])
        hbuf[:, cols] = (silu(gate) * up).astype(BF16)
        return carry

    lax.fori_loop(0, eg.shape[1] // tile, hidden_tile, 0)

    def expert_out(i):
        return dot(hbuf[...], ed[:, lanes(i)]).reshape(n_ep, PAD, quarter)

    y_copies = []
    for i in range(1, n_x):
        yb[i] = expert_out(i).astype(BF16)
        y_copies.append(
            remote(
                yb.at[i, :, pl.ds(0, ROWS)],
                yr.at[i, :, pl.ds(0, ROWS)],
                x_send.at[3, i],
                x_recv.at[3, i],
                x_peer(i),
            )
        )
        y_copies[-1].start()
    own_out = expert_out(0).astype(BF16).astype(F32)

    for i, copy in zip(range(1, n_x), rs2_copies):
        copy.wait_recv()
        paired = paired + rs2[i].astype(F32)
    hidden = (silu(paired[:, :all_units]) * paired[:, all_units:]).astype(BF16)
    block = pl.ds(x * per_x, per_x)
    hid_all[block] = hidden.reshape(per_x, tokens, all_units)
    h_copies = [
        remote(
            hid_all.at[block], hid_all.at[block], x_send.at[4, i], x_recv.at[4, i], x_peer(i)
        )
        for i in range(1, n_x)
    ]
    for copy in h_copies:
        copy.start()

    for i, copy in zip(range(1, n_x), y_copies):
        copy.wait_recv()
        own_out = own_out + yr[i].astype(F32)
    rb[...] = own_out.astype(BF16)

    def send_home(i, carry):
        to = lax.rem(ep + i, n_ep)
        remote(
            rb.at[to, pl.ds(0, ROWS)],
            ret.at[ep, pl.ds(0, ROWS)],
            pl_send.at[1],
            pl_recv.at[1],
            (to, x),
        ).start()
        return carry

    lax.fori_loop(1, n_ep, send_home, 0)
    ret[pl.ds(ep, 1)] = rb[pl.ds(ep, 1)]

    for copy in h_copies:
        copy.wait_recv()
    dense_part = dot(hid_all[...].reshape(n_yc * tokens, all_units), wd[...])
    db[...] = dense_part.reshape(n_yc, tokens, quarter).astype(BF16)
    db_copies = [
        remote(
            db.at[lax.rem(yc + i, n_yc)],
            dr.at[i],
            yc_send.at[1, i],
            yc_recv.at[1, i],
            yc_peer(i),
        )
        for i in range(1, n_yc)
    ]
    for copy in db_copies:
        copy.start()

    dense = db[pl.ds(yc, 1)][0].astype(F32)
    for i, copy in zip(range(1, n_yc), db_copies):
        copy.wait_recv()
        dense = dense + dr[i].astype(F32)
    home = ret.at[pl.ds(0, n_ep - 1), pl.ds(0, ROWS)]
    pltpu.make_async_copy(home, home, pl_recv.at[1]).wait()
    back = ret[...].reshape(flat, quarter)
    routed = dot(comb_hi_ref[...], back) + dot(comb_lo_ref[...], back)
    middle_own = mid[pl.ds(x, 1)][0].astype(F32)
    out_ref[...] = (middle_own + branch * dense + routed).astype(BF16)

    for copy in rs1_copies + mid_copies + rs2_copies + y_copies + h_copies:
        copy.wait_send()
    for copy in wz_copies + yc_copies + db_copies:
        copy.wait_send()
    sent = snd.at[pl.ds(0, n_ep - 1), pl.ds(0, ROWS)]
    pltpu.make_async_copy(sent, sent, pl_send.at[0]).wait()
    sent_home = rb.at[pl.ds(0, n_ep - 1), pl.ds(0, ROWS)]
    pltpu.make_async_copy(sent_home, sent_home, pl_send.at[1]).wait()


def branches(sizes, part, hid, gain, bgate, sel, comb_hi, comb_lo, eg, eu, ed, dg, du, dd):
    n_ep, n_x, n_z = sizes
    n_yc = n_ep // n_z
    tokens, width = hid.shape
    quarter, units = width // n_x, dg.shape[1]
    all_units = n_z * units
    flat = n_ep * PAD
    group_rows = n_yc * tokens // n_x
    vmem = pl.BlockSpec(memory_space=pltpu.VMEM)
    anyspace = pl.BlockSpec(memory_space=pltpu.HBM)
    dma = pltpu.SemaphoreType.DMA
    return pl.pallas_call(
        functools.partial(branches_kernel, sizes),
        name="branches",
        out_shape=jax.ShapeDtypeStruct((tokens, quarter), BF16),
        in_specs=[vmem] * 7 + [anyspace] * 6,
        out_specs=vmem,
        scratch_shapes=[
            pltpu.VMEM(eg.shape, BF16),
            pltpu.VMEM(eu.shape, BF16),
            pltpu.VMEM(ed.shape, BF16),
            pltpu.VMEM((quarter, 2 * all_units), BF16),
            pltpu.VMEM((all_units, quarter), BF16),
            pltpu.VMEM((n_x, tokens, quarter), BF16),
            pltpu.VMEM((n_x, tokens, quarter), BF16),
            pltpu.VMEM((n_ep, PAD, width), BF16),
            pltpu.VMEM((n_ep, PAD, width), BF16),
            pltpu.VMEM((n_yc, tokens, quarter), BF16),
            pltpu.VMEM((n_x, group_rows, 2 * all_units), BF16),
            pltpu.VMEM((n_x, group_rows, 2 * all_units), BF16),
            pltpu.VMEM((n_yc, tokens, all_units), BF16),
            pltpu.VMEM((n_yc, tokens, quarter), BF16),
            pltpu.VMEM((n_yc, tokens, quarter), BF16),
            pltpu.VMEM((flat, eg.shape[1]), BF16),
            pltpu.VMEM((n_x, n_ep, PAD, quarter), BF16),
            pltpu.VMEM((n_x, n_ep, PAD, quarter), BF16),
            pltpu.VMEM((n_ep, PAD, quarter), BF16),
            pltpu.VMEM((n_ep, PAD, quarter), BF16),
            dma((6,)),
            dma((n_z, 3)),
            dma((n_z, 3)),
            dma((5, n_x)),
            dma((5, n_x)),
            dma((2, n_yc)),
            dma((2, n_yc)),
            dma((2,)),
            dma((2,)),
        ],
        compiler_params=pltpu.CompilerParams(
            collective_id=0, has_side_effects=True, vmem_limit_bytes=48 << 20
        ),
    )(part, hid, gain, bgate, sel, comb_hi, comb_lo, eg, eu, ed, dg, du, dd)


def body(
    sizes,
    hidden_in,
    carried_state,
    input_gain,
    query_weight,
    key_weight,
    value_weight,
    outgate_weight,
    decay_weight,
    decay_shift,
    head_gain,
    output_weight,
    channel_gain,
    branch_gate,
    routes,
    route_weights,
    expert_gate,
    expert_up,
    expert_down,
    dense_gate,
    dense_up,
    dense_down,
):
    width = hidden_in.shape[1]
    part, new_state, sel, comb_hi, comb_lo = attention(
        sizes[0],
        hidden_in,
        input_gain.reshape(1, width),
        decay_shift,
        head_gain,
        routes,
        route_weights,
        (query_weight, key_weight, value_weight, outgate_weight, decay_weight),
        output_weight,
        carried_state[:, 0],
    )
    mixed = branches(
        sizes,
        part,
        hidden_in,
        channel_gain.reshape(1, width),
        branch_gate.reshape(1, width),
        sel,
        comb_hi,
        comb_lo,
        expert_gate[0],
        expert_up[0],
        expert_down[0],
        dense_gate,
        dense_up,
        dense_down,
    )
    return (mixed, new_state[:, None])


def solution(mesh):
    in_specs = (
        P("ep", None),
        P("ep", "tp", None, None),
        P(),
        P(None, "tp"),
        P(None, "tp"),
        P(None, "tp"),
        P(None, "tp"),
        P(None, "tp"),
        P("ep", "tp"),
        P("tp", None),
        P("tp", None),
        P(),
        P(),
        P("ep", None),
        P("ep", None),
        P("ep", None, "tp"),
        P("ep", None, "tp"),
        P("ep", "tp", None),
        P("tp", "ep"),
        P("tp", "ep"),
        P("ep", "tp"),
    )
    out_specs = (P("ep", "tp"), P("ep", "tp", None, None))
    n_ep = mesh.shape["ep"]
    sizes = (n_ep, mesh.shape["tp"], min(Z_SIZE, n_ep // 2))
    return jax.shard_map(
        functools.partial(body, sizes),
        mesh=mesh,
        in_specs=in_specs,
        out_specs=out_specs,
        check_vma=False,
    )
```

time: 169 us -> 89.1 us (0.53); the launches traced: 166 us -> 88.5 us
  Pallas kernels: 0 us -> 72.9 us
  waiting for transfers between devices: 51.5 us -> 0 us
  matrix products: 32.9 us -> 0 us
  starting transfers between devices: 26.2 us -> 0 us
  other arithmetic: 22.6 us -> 0 us
  between operations: 14.3 us -> 0.76 us
  local copies, waits for them, and re-layouts: 18.5 us -> 14.8 us
    pallas_call x0 -> x2, Pallas kernels: none -> 72.9 us  [the longest x1 65.5 us: branches(): pl.pallas_call(functools.partial(branches_kernel, sizes), name='branches'...]
    all_to_all x4 -> x0, waiting for transfers between devices: 39.2 us -> none  [the longest x1 23.4 us: body(): lax.all_to_all(outgoing, 'ep', split_axis=0, concat_axis=0, tiled=True)]
    dot_general x12 -> x0, matrix products: 32.9 us -> none  [the longest x11 29 us: matmul(): return jnp.dot(left, right, preferred_element_type=jnp.float32)]
    all_to_all x4 -> x0, starting transfers between devices: 26.1 us -> none  [the longest x1 10.3 us: body(): lax.all_to_all(outgoing, 'ep', split_axis=0, concat_axis=0, tiled=True)]
    psum x1 -> x0, waiting for transfers between devices: 12.3 us -> none  [unit_totals(): return lax.psum(paired.astype(jnp.bfloat16), 'tp').astype(jnp.float32)]
    unnamed x26 -> x37, local copies, waits for them, and re-layouts: 5.05 us -> 14.1 us
    reshape x7 -> x3, local copies, waits for them, and re-layouts: 8.42 us -> 0.71 us  [the longest x1 0.69 us: body(): input_gain.reshape(1, width)]
    add x1 -> x0, other arithmetic: 7.31 us -> none  [body(): decay[..., None] * carried_state]
  transfers between devices with their start and end apart: 6 -> 0, of which waited for: 4 -> 0; matrix products, arithmetic and copies ran while one was open for 39% -> 0% of each run, Pallas kernels for 0% -> 0%
where the time goes in v1:
time: 89.1 us; the launch traced here: 88.5 us
  Pallas kernels  72.9 us (82%)
  local copies, waits for them, and re-layouts  14.8 us (17%)
    pallas_call x1, Pallas kernels, branches(): pl.pallas_call(functools.partial(branches_kernel, sizes), name='branches'...  65.5 us
    unnamed x37, local copies, waits for them, and re-layouts  14.1 us
    pallas_call x1, Pallas kernels, attention(): pl.pallas_call(functools.partial(attention_kernel, experts), name='attent...  7.45 us

profile of v1, /device:TPU:1, one launch (start us, length us, event | category | flops | bytes accessed | tf_op | source)
XLA Modules:
  0.0 88.5 jit_solution(2609447819148315098)
XLA Ops:
  0.6 0.8 copy.23.routes_ref
  1.4 0.8 copy.24.rw_ref
  2.2 0.7 reshape.13.gain_ref
  2.9 0.0 copy-start
  2.9 2.8 %copy-done = f32[48,1,128,256]{3,2,1,0:T(8,128)S(1)} copy-done((f32[48,1,128,256]{3,2,1,0:T(8,128)S(1)}, f32[48,1,128,256]{3,2,1,0:T(8,128)}, u32[]{:S(2)}) %copy-start) | copy-done | bytes 6291480
  5.6 0.0 copy-start.2
  5.6 1.2 %copy-done.2 = bf16[2048,256]{1,0:T(8,128)(2,1)S(1)} copy-done((bf16[2048,256]{1,0:T(8,128)(2,1)S(1)}, bf16[2048,256]{1,0:T(8,128)(2,1)}, u32[]{:S(2)}) %copy-start.2) | copy-done | bytes 1048600
  6.9 0.0 copy-start.3
  6.9 1.2 %copy-done.3 = bf16[2048,256]{1,0:T(8,128)(2,1)S(1)} copy-done((bf16[2048,256]{1,0:T(8,128)(2,1)S(1)}, bf16[2048,256]{1,0:T(8,128)(2,1)}, u32[]{:S(2)}) %copy-start.3) | copy-done | bytes 1048600
  8.1 0.0 copy-start.4
  8.1 1.2 %copy-done.4 = bf16[256,2048]{1,0:T(8,128)(2,1)S(1)} copy-done((bf16[256,2048]{1,0:T(8,128)(2,1)S(1)}, bf16[256,2048]{1,0:T(8,128)(2,1)}, u32[]{:S(2)}) %copy-start.4) | copy-done | bytes 1048600
  9.3 0.0 copy-start.5
  9.3 0.9 %copy-done.5 = bf16[48,2048]{1,0:T(8,128)(2,1)S(1)} copy-done((bf16[48,2048]{1,0:T(8,128)(2,1)S(1)}, bf16[48,2048]{1,0:T(8,128)(2,1)}, u32[]{:S(2)}) %copy-start.5) | copy-done | bytes 196632
  10.2 0.0 copy-start.7
  10.2 1.0 %copy-done.7 = bf16[2048,128]{1,0:T(8,128)(2,1)S(1)} copy-done((bf16[2048,128]{1,0:T(8,128)(2,1)S(1)}, bf16[2048,128]{1,0:T(8,128)(2,1)}, u32[]{:S(2)}) %copy-start.7) | copy-done | bytes 524312
  11.3 0.0 copy-start.8
  11.3 1.0 %copy-done.8 = bf16[2048,128]{1,0:T(8,128)(2,1)S(1)} copy-done((bf16[2048,128]{1,0:T(8,128)(2,1)S(1)}, bf16[2048,128]{1,0:T(8,128)(2,1)}, u32[]{:S(2)}) %copy-start.8) | copy-done | bytes 524312
  12.3 0.0 copy-start.9
  12.3 1.0 %copy-done.9 = bf16[2048,128]{1,0:T(8,128)(2,1)S(1)} copy-done((bf16[2048,128]{1,0:T(8,128)(2,1)S(1)}, bf16[2048,128]{1,0:T(8,128)(2,1)}, u32[]{:S(2)}) %copy-start.9) | copy-done | bytes 524312
  13.4 0.0 copy-start.13
  13.4 0.7 copy-done.13
  14.1 0.0 copy-start.14
  14.1 0.7 copy-done.14
  14.8 0.0 copy-start.15
  14.8 0.0 copy-start.16
  14.8 0.0 copy-start.1
  14.8 0.0 copy-start.6
  14.8 0.0 copy-start.10
  14.8 0.0 copy-start.11
  14.8 0.0 copy-start.12
  14.8 7.4 %attention.1 = (bf16[48,2048]{1,0:T(8,128)(2,1)S(1)}, f32[48,128,256]{2,1,0:T(8,128)}, bf16[48,256]{1,0:T(8,128)(2,1)S(1)}, bf16[48,256]{1,0:T(8,128)(2,1)S(1)}, bf16[48,256]{1,0:T(8,128)(2,1)S(1)}) custom-call(bf16[48,2048]{1,0:T(8,128)(2,1)S(1)} %copy-done.5, bf16[1,2048]{1,0:T(2,128)(2,1)S(1)} %reshape.13.gain_ref, f32[48,128]{1,0:T(8,128)S(1)} %copy-done.13, ...), custom_call_target="tpu_custom_call" | custom-call | tf_op jit(solution)/shard_map/attention/pallas_call | solution.py:164
  22.3 0.0 copy-done.15
  22.3 0.0 copy-done.16
  22.3 0.0 copy-done.1
  22.3 0.0 copy-done.6
  22.4 0.0 copy-done.10
  22.4 0.0 copy-done.11
  22.4 0.0 copy-done.12
  22.4 65.5 %branches.1 = bf16[48,512]{1,0:T(8,128)(2,1)S(1)} custom-call(bf16[48,2048]{1,0:T(8,128)(2,1)S(1)} %get-tuple-element.7.part_ref, bf16[48,2048]{1,0:T(8,128)(2,1)S(1)} %copy-done.6, bf16[1,2048]{1,0:T(2,128)(2,1)S(1)} %reshape.14.gain_ref, bf16[1,2048]{1,0:T(2,128)(2,1)S(1)} %reshape.15.bgate_ref, bf16[48,256]{1,0:T(8,128)(2,1)S(1)} %get-tuple-element.8.sel_ref, ...), custom_call_target="tpu_custom_call" | custom-call | tf_op jit(solution)/shard_map/branches/pallas_call | solution.py:511
  87.9 0.6 copy.27
  (2 shorter events, 0.0 us)
Async XLA Ops:
  2.9 2.8 %copy-start = (f32[48,1,128,256]{3,2,1,0:T(8,128)S(1)}, f32[48,1,128,256]{3,2,1,0:T(8,128)}, u32[]{:S(2)}) copy-start(f32[48,1,128,256]{3,2,1,0:T(8,128)} %param.22) | copy-start | bytes 18874372
  5.6 1.2 %copy-start.2 = (bf16[2048,256]{1,0:T(8,128)(2,1)S(1)}, bf16[2048,256]{1,0:T(8,128)(2,1)}, u32[]{:S(2)}) copy-start(bf16[2048,256]{1,0:T(8,128)(2,1)} %vw_hbm.1) | copy-start | bytes 3145732
  6.9 1.2 %copy-start.3 = (bf16[2048,256]{1,0:T(8,128)(2,1)S(1)}, bf16[2048,256]{1,0:T(8,128)(2,1)}, u32[]{:S(2)}) copy-start(bf16[2048,256]{1,0:T(8,128)(2,1)} %ow_hbm.1) | copy-start | bytes 3145732
  8.1 1.2 %copy-start.4 = (bf16[256,2048]{1,0:T(8,128)(2,1)S(1)}, bf16[256,2048]{1,0:T(8,128)(2,1)}, u32[]{:S(2)}) copy-start(bf16[256,2048]{1,0:T(8,128)(2,1)} %pw_hbm.1) | copy-start | bytes 3145732
  9.3 0.9 %copy-start.5 = (bf16[48,2048]{1,0:T(8,128)(2,1)S(1)}, bf16[48,2048]{1,0:T(8,128)(2,1)}, u32[]{:S(2)}) copy-start(bf16[48,2048]{1,0:T(8,128)(2,1)} %hid_ref.3) | copy-start | bytes 589828
  10.2 1.0 %copy-start.7 = (bf16[2048,128]{1,0:T(8,128)(2,1)S(1)}, bf16[2048,128]{1,0:T(8,128)(2,1)}, u32[]{:S(2)}) copy-start(bf16[2048,128]{1,0:T(8,128)(2,1)} %qw_hbm.1) | copy-start | bytes 1572868
  11.3 1.0 %copy-start.8 = (bf16[2048,128]{1,0:T(8,128)(2,1)S(1)}, bf16[2048,128]{1,0:T(8,128)(2,1)}, u32[]{:S(2)}) copy-start(bf16[2048,128]{1,0:T(8,128)(2,1)} %kw_hbm.1) | copy-start | bytes 1572868
  12.3 1.0 %copy-start.9 = (bf16[2048,128]{1,0:T(8,128)(2,1)S(1)}, bf16[2048,128]{1,0:T(8,128)(2,1)}, u32[]{:S(2)}) copy-start(bf16[2048,128]{1,0:T(8,128)(2,1)} %dw_hbm.1) | copy-start | bytes 1572868
  13.4 0.7 copy-start.13
  14.1 0.7 copy-start.14
  14.8 7.5 %copy-start.15 = (bf16[2048]{0:T(1024)(128)(2,1)S(1)}, bf16[2048]{0:T(1024)(128)(2,1)}, u32[]{:S(2)}) copy-start(bf16[2048]{0:T(1024)(128)(2,1)} %param.32) | copy-start | bytes 12292
  14.8 7.5 %copy-start.16 = (bf16[2048]{0:T(1024)(128)(2,1)S(1)}, bf16[2048]{0:T(1024)(128)(2,1)}, u32[]{:S(2)}) copy-start(bf16[2048]{0:T(1024)(128)(2,1)} %param.33) | copy-start | bytes 12292
  14.8 7.6 %copy-start.1 = (bf16[1,2048,768]{2,1,0:T(8,128)(2,1)S(1)}, bf16[1,2048,768]{2,1,0:T(8,128)(2,1)}, u32[]{:S(2)}) copy-start(bf16[1,2048,768]{2,1,0:T(8,128)(2,1)} %param.36) | copy-start | bytes 9437188
  14.8 7.6 %copy-start.6 = (bf16[48,2048]{1,0:T(8,128)(2,1)S(1)}, bf16[48,2048]{1,0:T(8,128)(2,1)}, u32[]{:S(2)}) copy-start(bf16[48,2048]{1,0:T(8,128)(2,1)} %hid_ref.3) | copy-start | bytes 589828
  14.8 7.6 %copy-start.10 = (bf16[512,128]{1,0:T(8,128)(2,1)S(1)}, bf16[512,128]{1,0:T(8,128)(2,1)}, u32[]{:S(2)}) copy-start(bf16[512,128]{1,0:T(8,128)(2,1)} %dg_hbm.1) | copy-start | bytes 393220
  14.8 7.6 %copy-start.11 = (bf16[512,128]{1,0:T(8,128)(2,1)S(1)}, bf16[512,128]{1,0:T(8,128)(2,1)}, u32[]{:S(2)}) copy-start(bf16[512,128]{1,0:T(8,128)(2,1)} %du_hbm.1) | copy-start | bytes 393220
  14.8 7.6 %copy-start.12 = (bf16[128,512]{1,0:T(8,128)(2,1)S(1)}, bf16[128,512]{1,0:T(8,128)(2,1)}, u32[]{:S(2)}) copy-start(bf16[128,512]{1,0:T(8,128)(2,1)} %dd_hbm.1) | copy-start | bytes 393220

commit v2 on v1

--- a/solution.py
+++ b/solution.py
@@ -12,6 +12,7 @@
 MESH = pl.DeviceIdType.MESH
 CAP = 5
 ROWS = 6
+VMEM_ALL = 67043328
 PAD = 8
 Z_SIZE = 4
 F32 = jnp.float32
@@ -22,6 +23,14 @@
     return jnp.dot(left, right, preferred_element_type=F32)
 
 
+def in_hbm(*arrays):
+    return [pltpu.with_memory_space_constraint(a, pltpu.HBM) for a in arrays]
+
+
+def turned_dot(left, right):
+    return lax.dot_general(left, right, (((0,), (0,)), ((), ())), preferred_element_type=F32)
+
+
 def rms_factor(values):
     return lax.rsqrt(jnp.mean(values * values, axis=-1, keepdims=True) + EPSILON)
 
@@ -32,12 +41,12 @@
 
 def attention_kernel(
     experts,
-    hid_ref,
-    gain_ref,
-    shift_ref,
-    hgain_ref,
-    routes_ref,
-    rw_ref,
+    routes_hbm,
+    rw_hbm,
+    hid_hbm,
+    gain_hbm,
+    shift_hbm,
+    hgain_hbm,
     qw_hbm,
     kw_hbm,
     vw_hbm,
@@ -50,6 +59,12 @@
     sel_ref,
     comb_hi_ref,
     comb_lo_ref,
+    routes_s,
+    rw_s,
+    hid_s,
+    gain_s,
+    shift_s,
+    hgain_s,
     qw,
     kw,
     vw,
@@ -68,6 +83,17 @@
 ):
     tokens, key_dim = q_s.shape
     groups = tokens // 8
+    small = (
+        (routes_hbm, routes_s),
+        (rw_hbm, rw_s),
+        (hid_hbm, hid_s),
+        (gain_hbm, gain_s),
+        (shift_hbm, shift_s),
+        (hgain_hbm, hgain_s),
+    )
+    s_copies = [pltpu.make_async_copy(s, d, w_sem.at[6 + i]) for i, (s, d) in enumerate(small)]
+    for copy in s_copies:
+        copy.start()
     pairs = ((dw_hbm, dw), (qw_hbm, qw), (kw_hbm, kw), (vw_hbm, vw))
     w_copies = [pltpu.make_async_copy(s, d, w_sem.at[i]) for i, (s, d) in enumerate(pairs)]
     for copy in w_copies:
@@ -88,34 +114,38 @@
     p_copy = pltpu.make_async_copy(pw_hbm, pw, w_sem.at[5])
     p_copy.start()
 
+    for copy in s_copies[:2]:
+        copy.wait()
     slots = experts * PAD
-    e_at = lax.broadcasted_iota(jnp.int32, (tokens, experts), 1)
-    r0, r1 = routes_ref[:, 0:1], routes_ref[:, 1:2]
+    e_at = lax.broadcasted_iota(jnp.int32, (experts, tokens), 0)
+    r0, r1 = routes_s[0:1, :], routes_s[1:2, :]
     oh0, oh1 = (e_at == r0).astype(F32), (e_at == r1).astype(F32)
     tri = (
         lax.broadcasted_iota(jnp.int32, (tokens, tokens), 0)
-        > lax.broadcasted_iota(jnp.int32, (tokens, tokens), 1)
+        < lax.broadcasted_iota(jnp.int32, (tokens, tokens), 1)
     ).astype(F32)
-    before0 = dot(tri, oh0)
-    before1 = dot(tri, oh1) + jnp.sum(oh0, axis=0, keepdims=True)
-    slot0 = jnp.sum(before0 * oh0, axis=1, keepdims=True)
-    slot1 = jnp.sum(before1 * oh1, axis=1, keepdims=True)
+    before0 = dot(oh0, tri)
+    before1 = dot(oh1, tri) + jnp.sum(oh0, axis=1, keepdims=True)
+    slot0 = jnp.sum(before0 * oh0, axis=0, keepdims=True)
+    slot1 = jnp.sum(before1 * oh1, axis=0, keepdims=True)
     pos0 = r0 * PAD + slot0.astype(jnp.int32)
     pos1 = r1 * PAD + slot1.astype(jnp.int32)
-    at = lax.broadcasted_iota(jnp.int32, (tokens, slots), 1)
+    at = lax.broadcasted_iota(jnp.int32, (slots, tokens), 0)
     hit0, hit1 = (at == pos0).astype(F32), (at == pos1).astype(F32)
     sel_ref[...] = (hit0 + hit1).astype(BF16)
-    comb = hit0 * rw_ref[:, 0:1] + hit1 * rw_ref[:, 1:2]
+    comb = hit0 * rw_s[0:1, :] + hit1 * rw_s[1:2, :]
     comb_hi = comb.astype(BF16)
     comb_hi_ref[...] = comb_hi
     comb_lo_ref[...] = (comb - comb_hi.astype(F32)).astype(BF16)
 
-    hid = hid_ref[...].astype(F32)
-    normed = (hid * rms_factor(hid) * gain_ref[...].astype(F32)).astype(BF16)
+    for copy in s_copies[2:]:
+        copy.wait()
+    hid = hid_s[...].astype(F32)
+    normed = (hid * rms_factor(hid) * gain_s[...][None, :].astype(F32)).astype(BF16)
     w_copies[0].wait()
     pre = dot(normed, dw[...])
     log_sig = jnp.minimum(pre, 0.0) - jnp.log1p(jnp.exp(-jnp.abs(pre)))
-    d_s[...] = jnp.exp(log_sig / TAU_DECAY + shift_ref[...])
+    d_s[...] = jnp.exp(log_sig / TAU_DECAY + shift_s[...])
     w_copies[1].wait()
     q_s[...] = dot(normed, qw[...]).astype(BF16).astype(F32) * key_dim ** (-0.5)
     w_copies[2].wait()
@@ -146,7 +176,7 @@
     o_copy.wait()
     outgate = dot(normed, ow[...]).astype(BF16).astype(F32)
     readout = ro_s[...]
-    gated = readout * rms_factor(readout) * hgain_ref[...].astype(F32) * silu(outgate)
+    gated = readout * rms_factor(readout) * hgain_s[...].astype(F32) * silu(outgate)
     state_back(groups - 1).start()
     p_copy.wait()
     part_ref[...] = dot(gated.astype(BF16), pw[...]).astype(BF16)
@@ -167,13 +197,16 @@
         out_shape=(
             jax.ShapeDtypeStruct((tokens, width), BF16),
             jax.ShapeDtypeStruct(state.shape, F32),
-            jax.ShapeDtypeStruct((tokens, slots), BF16),
-            jax.ShapeDtypeStruct((tokens, slots), BF16),
-            jax.ShapeDtypeStruct((tokens, slots), BF16),
+            jax.ShapeDtypeStruct((slots, tokens), BF16),
+            jax.ShapeDtypeStruct((slots, tokens), BF16),
+            jax.ShapeDtypeStruct((slots, tokens), BF16),
         ),
-        in_specs=[vmem] * 6 + [anyspace] * 7,
+        in_specs=[anyspace] * 13,
         out_specs=(vmem, anyspace, vmem, vmem, vmem),
-        scratch_shapes=[pltpu.VMEM(w.shape, BF16) for w in weights]
+        scratch_shapes=[
+            pltpu.VMEM(a.shape, a.dtype)
+            for a in (routes, rw, hid, gain, shift, hgain) + tuple(weights)
+        ]
         + [
             pltpu.VMEM(pw.shape, BF16),
             pltpu.VMEM(state.shape, F32),
@@ -182,12 +215,12 @@
             pltpu.VMEM((tokens, value_dim), F32),
             pltpu.VMEM((tokens, key_dim), F32),
             pltpu.VMEM((tokens, value_dim), F32),
-            pltpu.SemaphoreType.DMA((6,)),
+            pltpu.SemaphoreType.DMA((12,)),
             pltpu.SemaphoreType.DMA((groups,)),
             pltpu.SemaphoreType.DMA((groups,)),
         ],
         compiler_params=pltpu.CompilerParams(vmem_limit_bytes=40 << 20),
-    )(hid, gain, shift, hgain, routes, rw, *weights, pw, state)
+    )(*in_hbm(routes, rw, hid, gain, shift, hgain, *weights, pw, state))
 
 
 def branches_kernel(
@@ -335,7 +368,7 @@
         jnp.sum(mid[i].astype(F32) * mid[i].astype(F32), axis=-1, keepdims=True) for i in range(n_x)
     )
     factor = lax.rsqrt(squares / width + EPSILON)
-    own_scaled = mid[pl.ds(x, 1)][0].astype(F32) * factor * gain_ref[:, lanes(0)].astype(F32)
+    own_scaled = mid[pl.ds(x, 1)][0].astype(F32) * factor * gain_ref[lanes(0)][None, :].astype(F32)
     ffn_all[pl.ds(yc, 1)] = own_scaled.astype(BF16)[None]
     yc_copies = [
         remote(
@@ -348,11 +381,9 @@
     logit = jnp.zeros((tokens, 1), F32)
     for i in range(n_x):
         part = slice(i * quarter, (i + 1) * quarter)
-        scaled = mid[i].astype(F32) * factor * gain_ref[:, part].astype(F32)
-        logit = logit + jnp.sum(scaled * bgate_ref[:, part].astype(F32), axis=-1, keepdims=True)
-        rows = lax.dot_general(
-            sel_ref[...], scaled.astype(BF16), (((0,), (0,)), ((), ())), preferred_element_type=F32
-        )
+        scaled = mid[i].astype(F32) * factor * gain_ref[part][None, :].astype(F32)
+        logit = logit + jnp.sum(scaled * bgate_ref[part][None, :].astype(F32), axis=-1, keepdims=True)
+        rows = dot(sel_ref[...], scaled.astype(BF16))
         snd[:, :, part] = rows.reshape(n_ep, PAD, quarter).astype(BF16)
     branch = jax.nn.sigmoid(logit)
 
@@ -483,7 +514,7 @@
     home = ret.at[pl.ds(0, n_ep - 1), pl.ds(0, ROWS)]
     pltpu.make_async_copy(home, home, pl_recv.at[1]).wait()
     back = ret[...].reshape(flat, quarter)
-    routed = dot(comb_hi_ref[...], back) + dot(comb_lo_ref[...], back)
+    routed = turned_dot(comb_hi_ref[...], back) + turned_dot(comb_lo_ref[...], back)
     middle_own = mid[pl.ds(x, 1)][0].astype(F32)
     out_ref[...] = (middle_own + branch * dense + routed).astype(BF16)
 
@@ -548,7 +579,7 @@
         compiler_params=pltpu.CompilerParams(
             collective_id=0, has_side_effects=True, vmem_limit_bytes=48 << 20
         ),
-    )(part, hid, gain, bgate, sel, comb_hi, comb_lo, eg, eu, ed, dg, du, dd)
+    )(part, hid, gain, bgate, sel, comb_hi, comb_lo, *in_hbm(eg, eu, ed, dg, du, dd))
 
 
 def body(
@@ -575,15 +606,14 @@
     dense_up,
     dense_down,
 ):
-    width = hidden_in.shape[1]
     part, new_state, sel, comb_hi, comb_lo = attention(
         sizes[0],
         hidden_in,
-        input_gain.reshape(1, width),
+        input_gain,
         decay_shift,
         head_gain,
-        routes,
-        route_weights,
+        routes.T,
+        route_weights.T,
         (query_weight, key_weight, value_weight, outgate_weight, decay_weight),
         output_weight,
         carried_state[:, 0],
@@ -592,8 +622,8 @@
         sizes,
         part,
         hidden_in,
-        channel_gain.reshape(1, width),
-        branch_gate.reshape(1, width),
+        channel_gain,
+        branch_gate,
         sel,
         comb_hi,
         comb_lo,

time: 89.1 us -> 75.7 us (0.85)
  local copies, waits for them, and re-layouts: 14.8 us -> 0.64 us
  Pallas kernels: 72.9 us -> 74.2 us
    unnamed x37 -> x7, local copies, waits for them, and re-layouts: 14.1 us -> 0.64 us
    pallas_call x1, Pallas kernels: 7.45 us -> 8.51 us  [attention(): pl.pallas_call(functools.partial(attention_kernel, experts), name='attent...]
where the time goes in v2:
time: 75.7 us; the launch traced here: 75.6 us
  Pallas kernels  74.2 us (98%)
    pallas_call x1, Pallas kernels, branches(): pl.pallas_call(functools.partial(branches_kernel, sizes), name='branches'...  65.7 us
    pallas_call x1, Pallas kernels, attention(): pl.pallas_call(functools.partial(attention_kernel, experts), name='attent...  8.51 us

profile of v2, /device:TPU:1, one launch (start us, length us, event | category | flops | bytes accessed | tf_op | source)
XLA Modules:
  0.0 75.6 jit_solution(12158810588778419372)
XLA Ops:
  0.6 0.0 copy-start
  0.6 0.0 copy-start.1
  0.7 0.0 copy-start.2
  0.7 8.5 %attention.1 = (bf16[48,2048]{1,0:T(8,128)(2,1)S(1)}, f32[48,128,256]{2,1,0:T(8,128)}, bf16[256,48]{1,0:T(8,128)(2,1)S(1)}, bf16[256,48]{1,0:T(8,128)(2,1)S(1)}, bf16[256,48]{1,0:T(8,128)(2,1)S(1)}) custom-call(s32[2,48]{1,0:T(2,128)} %bitcast.13, f32[2,48]{1,0:T(2,128)} %bitcast.14, bf16[48,2048]{1,0:T(8,128)(2,1)} %hid_ref.1, bf16[2048]{0:T(1024)(128)(2,1)} %gain_hbm.1, ...), custom_call_target="tpu_custom_call" | custom-call | tf_op jit(solution)/shard_map/attention/pallas_call | solution.py:194
  9.2 0.0 copy-done
  9.2 0.0 copy-done.1
  9.2 0.0 copy-done.2
  9.2 65.7 %branches.1 = bf16[48,512]{1,0:T(8,128)(2,1)S(1)} custom-call(bf16[48,2048]{1,0:T(8,128)(2,1)S(1)} %get-tuple-element.7.part_ref, bf16[48,2048]{1,0:T(8,128)(2,1)S(1)} %copy-done, bf16[2048]{0:T(1024)(128)(2,1)S(1)} %copy-done.1, bf16[2048]{0:T(1024)(128)(2,1)S(1)} %copy-done.2, bf16[256,48]{1,0:T(8,128)(2,1)S(1)} %get-tuple-element.8.sel_ref, ...), custom_call_target="tpu_custom_call" | custom-call | tf_op jit(solution)/shard_map/branches/pallas_call | solution.py:542
  75.0 0.6 copy.25
Async XLA Ops:
  0.6 8.6 %copy-start = (bf16[48,2048]{1,0:T(8,128)(2,1)S(1)}, bf16[48,2048]{1,0:T(8,128)(2,1)}, u32[]{:S(2)}) copy-start(bf16[48,2048]{1,0:T(8,128)(2,1)} %hid_ref.1) | copy-start | bytes 589828
  0.6 8.6 %copy-start.1 = (bf16[2048]{0:T(1024)(128)(2,1)S(1)}, bf16[2048]{0:T(1024)(128)(2,1)}, u32[]{:S(2)}) copy-start(bf16[2048]{0:T(1024)(128)(2,1)} %gain_ref.1) | copy-start | bytes 12292
  0.7 8.6 %copy-start.2 = (bf16[2048]{0:T(1024)(128)(2,1)S(1)}, bf16[2048]{0:T(1024)(128)(2,1)}, u32[]{:S(2)}) copy-start(bf16[2048]{0:T(1024)(128)(2,1)} %bgate_ref.1) | copy-start | bytes 12292

commit v3 on v0

v3 whole, which is shorter than its diff:
```python
import functools

import jax
import jax.numpy as jnp
from jax import lax
from jax.experimental import pallas as pl
from jax.experimental.pallas import tpu as pltpu
from jax.sharding import PartitionSpec as P

EPSILON = 1e-06
TAU_DECAY = 16.0
MESH = pl.DeviceIdType.MESH
CAP = 5
ROWS = 6
VMEM_ALL = 67043328
PAD = 8
CHUNKS = 4
EARLY = 2
FLIGHT = 2
Z_SIZE = 4
F32 = jnp.float32
BF16 = jnp.bfloat16


def dot(left, right):
    return jnp.dot(left, right, preferred_element_type=F32)


def in_hbm(*arrays):
    return [pltpu.with_memory_space_constraint(a, pltpu.HBM) for a in arrays]


def turned_dot(left, right):
    return lax.dot_general(left, right, (((0,), (0,)), ((), ())), preferred_element_type=F32)


def rms_factor(values):
    return lax.rsqrt(jnp.mean(values * values, axis=-1, keepdims=True) + EPSILON)


def silu(values):
    return values * jax.nn.sigmoid(values)


def layer_kernel(
    sizes,
    routes_hbm,
    rw_hbm,
    hid_hbm,
    gain_hbm,
    shift_hbm,
    hgain_hbm,
    cgain_hbm,
    bgate_hbm,
    qw_hbm,
    kw_hbm,
    vw_hbm,
    ow_hbm,
    dw_hbm,
    pw_hbm,
    state_hbm,
    eg_hbm,
    eu_hbm,
    ed_hbm,
    dg_hbm,
    du_hbm,
    dd_hbm,
    out_ref,
    state_out,
    routes_s,
    rw_s,
    hid_s,
    gain_s,
    shift_s,
    hgain_s,
    cgain_s,
    bgate_s,
    qw,
    kw,
    vw,
    ow,
    dw,
    pw,
    q_s,
    k_s,
    v_s,
    d_s,
    ro_s,
    part,
    sel_ref,
    comb_hi_ref,
    comb_lo_ref,
    eg,
    eu,
    ed,
    wgu,
    wd,
    rs1,
    mid,
    snd,
    rcv,
    mid_all,
    ffn,
    fac,
    pr,
    rs2,
    hid_all,
    db,
    dr,
    yb,
    yr,
    rb,
    ret,
    w_sem,
    in_sem,
    local_sem,
    wz_send,
    wz_recv,
    x_send,
    x_recv,
    r_send,
    r_recv,
    y_send,
    y_recv,
    yc_send,
    yc_recv,
    pl_send,
    pl_recv,
):
    n_ep, n_x, n_z = sizes
    n_yc = n_ep // n_z
    n_y = n_yc // 2
    tokens, width = hid_s.shape
    key_dim = q_s.shape[1]
    groups = tokens // 8
    quarter = width // n_x
    units = dg_hbm.shape[1]
    all_units = n_z * units
    per_chunk = n_ep // CHUNKS
    ep, x = lax.axis_index("ep"), lax.axis_index("tp")
    z, yc = ep // n_yc, ep % n_yc
    y, c = yc // 2, yc % 2

    def x_peer(i):
        return (ep, lax.rem(x + i, n_x))

    def z_peer(i):
        return (lax.rem(z + i, n_z) * n_yc + yc, x)

    def yc_peer(i):
        return (z * n_yc + lax.rem(yc + i, n_yc), x)

    def offsets(r):
        k, j = r // per_chunk, r % per_chunk
        return j // 2, (j % 2) * 2 + k % 2, k // 2

    def ep_at(r, sign):
        dz, dy, dc = offsets(r)
        there_z = lax.rem(z + n_z + sign * dz, n_z)
        there_y = lax.rem(y + n_y + sign * dy, n_y)
        return (there_z * n_yc + there_y * 2 + lax.rem(c + dc, 2), x)

    def remote(src, dst, send, recv, device):
        return pltpu.make_async_remote_copy(
            src_ref=src,
            dst_ref=dst,
            send_sem=send,
            recv_sem=recv,
            device_id=device,
            device_id_type=MESH,
        )

    def lanes(i):
        return pl.ds(pl.multiple_of(lax.rem(x + i, n_x) * quarter, quarter), quarter)

    peers_x, peers_z, peers_yc = pl.ds(1, n_x - 1), pl.ds(1, n_z - 1), pl.ds(1, n_yc - 1)

    def wait_bytes(ref, sem):
        pltpu.make_async_copy(ref, ref, sem).wait()

    small = (
        (routes_hbm, routes_s),
        (rw_hbm, rw_s),
        (hid_hbm, hid_s),
        (gain_hbm, gain_s),
        (shift_hbm, shift_s),
        (hgain_hbm, hgain_s),
        (cgain_hbm, cgain_s),
        (bgate_hbm, bgate_s),
    )
    s_copies = [pltpu.make_async_copy(s, d, w_sem.at[6 + i]) for i, (s, d) in enumerate(small)]
    pairs = ((dw_hbm, dw), (qw_hbm, qw), (kw_hbm, kw), (vw_hbm, vw), (ow_hbm, ow), (pw_hbm, pw))
    w_copies = [pltpu.make_async_copy(s, d, w_sem.at[i]) for i, (s, d) in enumerate(pairs)]
    for copy in s_copies + w_copies[:4]:
        copy.start()

    def state_in(g):
        rows = pl.ds(g * 8, 8)
        return pltpu.make_async_copy(state_hbm.at[rows], state_out.at[rows], in_sem.at[g])

    places = ((dg_hbm, wgu.at[0, 0]), (du_hbm, wgu.at[0, 1]), (dd_hbm, wd.at[0]))
    d_copies = [
        pltpu.make_async_copy(s, d, local_sem.at[3 + i]) for i, (s, d) in enumerate(places)
    ]
    e_copies = [
        pltpu.make_async_copy(s, d, local_sem.at[i])
        for i, (s, d) in enumerate(((eg_hbm, eg), (eu_hbm, eu), (ed_hbm, ed)))
    ]

    rcv[...] = jnp.zeros_like(rcv)
    ret[...] = jnp.zeros_like(ret)
    barrier = pltpu.get_barrier_semaphore()
    for i in range(1, n_x):
        pl.semaphore_signal(barrier, inc=1, device_id=x_peer(i), device_id_type=MESH)
    for r in range(1, n_ep):
        pl.semaphore_signal(barrier, inc=1, device_id=ep_at(r, 1), device_id_type=MESH)
    for copy in d_copies:
        copy.start()
    for g in range(groups):
        state_in(g).start()
    for copy in w_copies[4:] + e_copies:
        copy.start()

    for copy in s_copies[:2]:
        copy.wait()
    slots = n_ep * PAD
    e_at = lax.broadcasted_iota(jnp.int32, (n_ep, tokens), 0)
    r0, r1 = routes_s[0:1, :], routes_s[1:2, :]
    oh0, oh1 = (e_at == r0).astype(F32), (e_at == r1).astype(F32)
    tri = (
        lax.broadcasted_iota(jnp.int32, (tokens, tokens), 0)
        < lax.broadcasted_iota(jnp.int32, (tokens, tokens), 1)
    ).astype(F32)
    before0 = dot(oh0, tri)
    before1 = dot(oh1, tri) + jnp.sum(oh0, axis=1, keepdims=True)
    slot0 = jnp.sum(before0 * oh0, axis=0, keepdims=True)
    slot1 = jnp.sum(before1 * oh1, axis=0, keepdims=True)

    def place_of(route):
        dz = ((route >> 3) - z) & 3
        dy = (((route >> 1) & 3) - y) & 3
        dc = ((route & 1) - c) & 1
        return (dc * 2 + (dy & 1)) * per_chunk + dz * 2 + (dy >> 1)

    pos0 = place_of(r0) * PAD + slot0.astype(jnp.int32)
    pos1 = place_of(r1) * PAD + slot1.astype(jnp.int32)
    at = lax.broadcasted_iota(jnp.int32, (slots, tokens), 0)
    hit0, hit1 = (at == pos0).astype(F32), (at == pos1).astype(F32)
    sel_ref[...] = (hit0 + hit1).astype(BF16)
    comb = hit0 * rw_s[0:1, :] + hit1 * rw_s[1:2, :]
    comb_hi = comb.astype(BF16)
    comb_hi_ref[...] = comb_hi
    comb_lo_ref[...] = (comb - comb_hi.astype(F32)).astype(BF16)

    for copy in d_copies:
        copy.wait()
    pl.semaphore_wait(barrier, n_x - 1 + n_ep - 1)
    near_first = [1, n_z - 1] + list(range(2, n_z - 1))
    for i in near_first:
        b = n_z - i
        remote(wgu.at[0], wgu.at[b], wz_send.at[0], wz_recv.at[b], z_peer(i)).start()

    for copy in s_copies[2:]:
        copy.wait()
    hid = hid_s[...].astype(F32)
    normed = (hid * rms_factor(hid) * gain_s[...][None, :].astype(F32)).astype(BF16)
    w_copies[0].wait()
    pre = dot(normed, dw[...])
    log_sig = jnp.minimum(pre, 0.0) - jnp.log1p(jnp.exp(-jnp.abs(pre)))
    d_s[...] = jnp.exp(log_sig / TAU_DECAY + shift_s[...])
    w_copies[1].wait()
    q_s[...] = dot(normed, qw[...]).astype(BF16).astype(F32) * key_dim ** (-0.5)
    w_copies[2].wait()
    k_s[...] = dot(normed, kw[...]).astype(BF16).astype(F32)
    w_copies[3].wait()
    v_s[...] = dot(normed, vw[...]).astype(BF16).astype(F32)

    def group(g, carry):
        state_in(g).wait()
        rows = pl.ds(pl.multiple_of(g * 8, 8), 8)
        d_t, k_t, q_t = d_s[rows, :].T, k_s[rows, :].T, q_s[rows, :].T
        v_8 = v_s[rows, :]
        outs = []
        for j in range(8):
            b = g * 8 + j
            new = d_t[:, j : j + 1] * state_out[b] + k_t[:, j : j + 1] * v_8[j : j + 1, :]
            state_out[b] = new
            outs.append(jnp.sum(q_t[:, j : j + 1] * new, axis=0, keepdims=True))
        ro_s[rows, :] = jnp.concatenate(outs, axis=0)
        return carry

    lax.fori_loop(0, groups, group, 0)

    w_copies[4].wait()
    outgate = dot(normed, ow[...]).astype(BF16).astype(F32)
    readout = ro_s[...]
    gated = readout * rms_factor(readout) * hgain_s[...].astype(F32) * silu(outgate)
    gated = gated.astype(BF16)
    w_copies[5].wait()

    for i in range(1, n_x):
        part[i] = dot(gated, pw[:, lanes(i)]).astype(BF16)
        remote(part.at[i], rs1.at[i], x_send.at[0], x_recv.at[0], x_peer(i)).start()
    total = dot(gated, pw[:, lanes(0)]).astype(BF16).astype(F32)

    wait_bytes(rs1.at[peers_x], x_recv.at[0])
    for i in range(1, n_x):
        total = total + rs1[i].astype(F32)
    middle_q = (hid_s[:, lanes(0)].astype(F32) + total).astype(BF16)
    mid[pl.ds(x, 1)] = middle_q[None]
    mid_all[pl.ds(yc, 1)] = middle_q[None]

    for i in range(1, n_x):
        remote(mid.at[x], mid.at[x], x_send.at[1], x_recv.at[1], x_peer(i)).start()
    for i in range(1, n_yc):
        remote(mid_all.at[yc], mid_all.at[yc], yc_send.at[0], yc_recv.at[0], yc_peer(i)).start()

    wait_bytes(mid.at[peers_x], x_recv.at[1])

    squares = sum(
        jnp.sum(mid[i].astype(F32) * mid[i].astype(F32), axis=-1, keepdims=True) for i in range(n_x)
    )
    factor = lax.rsqrt(squares / width + EPSILON)
    logit = jnp.zeros((tokens, 1), F32)
    for i in range(n_x):
        cols = slice(i * quarter, (i + 1) * quarter)
        scaled = mid[i].astype(F32) * factor * cgain_s[cols][None, :].astype(F32)
        logit = logit + jnp.sum(scaled * bgate_s[cols][None, :].astype(F32), axis=-1, keepdims=True)
        ffn[:, cols] = scaled.astype(BF16)
    branch = jax.nn.sigmoid(logit)

    def chunk(k):
        return pl.ds(k * per_chunk, per_chunk)

    def others(k):
        first = 1 if k == 0 else 0
        return pl.ds(k * per_chunk + first, per_chunk - first)

    def dispatch(k):
        for r in range(k * per_chunk, (k + 1) * per_chunk):
            if r:
                remote(
                    snd.at[r, pl.ds(0, ROWS)],
                    rcv.at[r, pl.ds(0, ROWS)],
                    pl_send.at[k],
                    pl_recv.at[k],
                    ep_at(r, 1),
                ).start()

    for k in range(CHUNKS):
        rows = dot(sel_ref[k * per_chunk * PAD : (k + 1) * per_chunk * PAD, :], ffn[...])
        snd[chunk(k)] = rows.reshape(per_chunk, PAD, width).astype(BF16)
        if k < FLIGHT:
            dispatch(k)
    rcv[0] = snd[0]
    factor_rows = jnp.broadcast_to(factor, (tokens, 128)).T[0:8, :]
    fac[pl.ds(yc, 1), :, 0:tokens] = factor_rows[None]
    for i in range(1, n_yc):
        remote(fac.at[yc], fac.at[yc], yc_send.at[2], yc_recv.at[2], yc_peer(i)).start()

    wait_bytes(mid_all.at[peers_yc], yc_recv.at[0])

    per_x = n_yc // n_x
    gain_q = cgain_s[lanes(0)][None, :].astype(F32)
    rows_in = mid_all[...].reshape(n_yc * tokens, quarter).astype(F32) * gain_q
    rows_in = rows_in.astype(BF16)

    def group_of(i):
        return pl.ds(lax.rem(x + i, n_x) * per_x, per_x)

    for b in [0] + near_first:
        if b:
            wait_bytes(wgu.at[b], wz_recv.at[b])
        paired = dot(rows_in, jnp.concatenate([wgu[b, 0], wgu[b, 1]], axis=1))
        pr[b] = paired.astype(BF16).reshape(n_yc, tokens, 2 * units)
        for i in range(1, n_x):
            remote(
                pr.at[b, group_of(i)], rs2.at[b, i], r_send.at[b], r_recv.at[b], x_peer(i)
            ).start()

    for copy in e_copies:
        copy.wait()
    flat = per_chunk * PAD

    def run_expert(k):
        wait_bytes(rcv.at[others(k), pl.ds(0, ROWS)], pl_recv.at[k])
        if k + FLIGHT < CHUNKS:
            dispatch(k + FLIGHT)
        rows = rcv[chunk(k)].reshape(flat, width)
        hidden = (silu(dot(rows, eg[...])) * dot(rows, eu[...])).astype(BF16)
        for i in list(range(1, n_x)) + [0]:
            out = dot(hidden, ed[:, lanes(i)])
            yb[k, i] = out.reshape(per_chunk, PAD, quarter).astype(BF16)
            if i:
                remote(
                    yb.at[k, i, :, pl.ds(0, ROWS)],
                    yr.at[k, i, :, pl.ds(0, ROWS)],
                    y_send.at[k],
                    y_recv.at[k],
                    x_peer(i),
                ).start()

    for k in range(EARLY):
        run_expert(k)

    wait_bytes(fac.at[peers_yc], yc_recv.at[2])
    factors = jnp.concatenate(
        [fac[pl.ds(x * per_x + b, 1)][0].T[0:tokens, 0:1] for b in range(per_x)], axis=0
    )
    group_rows = per_x * tokens
    for b in [0] + near_first:
        paired = pr[b, group_of(0)].reshape(group_rows, 2 * units).astype(F32)
        wait_bytes(rs2.at[b, peers_x], r_recv.at[b])
        for i in range(1, n_x):
            paired = paired + rs2[b, i].reshape(group_rows, 2 * units).astype(F32)
        gate, up = paired[:, :units] * factors, paired[:, units:] * factors
        hidden = (silu(gate) * up).astype(BF16)
        hid_all[group_of(0), :, b * units : (b + 1) * units] = hidden.reshape(per_x, tokens, units)
    for i in range(1, n_x):
        remote(
            hid_all.at[group_of(0)],
            hid_all.at[group_of(0)],
            x_send.at[2],
            x_recv.at[2],
            x_peer(i),
        ).start()
    for i in near_first:
        remote(wd.at[0], wd.at[n_z - i], wz_send.at[1], wz_recv.at[0], z_peer(i)).start()

    for k in range(EARLY, CHUNKS):
        run_expert(k)

    def go_home(k):
        out = yb[k, 0].astype(F32)
        wait_bytes(yr.at[k, peers_x, :, pl.ds(0, ROWS)], y_recv.at[k])
        for i in range(1, n_x):
            out = out + yr[k, i].astype(F32)
        rb[chunk(k)] = out.astype(BF16)
        for r in range(k * per_chunk, (k + 1) * per_chunk):
            if r:
                remote(
                    rb.at[r, pl.ds(0, ROWS)],
                    ret.at[r, pl.ds(0, ROWS)],
                    pl_send.at[CHUNKS],
                    pl_recv.at[CHUNKS],
                    ep_at(r, -1),
                ).start()
            else:
                ret[0] = rb[0]

    for k in range(EARLY):
        go_home(k)

    wait_bytes(hid_all.at[pl.ds(0, n_yc - per_x)], x_recv.at[2])

    wait_bytes(wd.at[peers_z], wz_recv.at[0])
    dense_part = dot(
        hid_all[...].reshape(n_yc * tokens, all_units), wd[...].reshape(all_units, quarter)
    )
    db[...] = dense_part.reshape(n_yc, tokens, quarter).astype(BF16)
    for i in range(1, n_yc):
        remote(
            db.at[lax.rem(yc + i, n_yc)], dr.at[i], yc_send.at[1], yc_recv.at[1], yc_peer(i)
        ).start()

    for k in range(EARLY, CHUNKS):
        go_home(k)

    dense = db[pl.ds(yc, 1)][0].astype(F32)
    wait_bytes(dr.at[peers_yc], yc_recv.at[1])
    for i in range(1, n_yc):
        dense = dense + dr[i].astype(F32)

    wait_bytes(ret.at[pl.ds(1, n_ep - 1), pl.ds(0, ROWS)], pl_recv.at[CHUNKS])

    back = ret[...].reshape(n_ep * PAD, quarter)
    routed = turned_dot(comb_hi_ref[...], back) + turned_dot(comb_lo_ref[...], back)
    middle_own = mid[pl.ds(x, 1)][0].astype(F32)
    out_ref[...] = (middle_own + branch * dense + routed).astype(BF16)

    wait_bytes(part.at[peers_x], x_send.at[0])
    wait_bytes(mid.at[peers_x], x_send.at[1])
    wait_bytes(hid_all.at[pl.ds(0, n_yc - per_x)], x_send.at[2])
    for b in range(n_z):
        wait_bytes(rs2.at[b, peers_x], r_send.at[b])
    for k in range(CHUNKS):
        wait_bytes(yb.at[k, peers_x, :, pl.ds(0, ROWS)], y_send.at[k])
    wait_bytes(wgu.at[peers_z], wz_send.at[0])
    wait_bytes(wd.at[peers_z], wz_send.at[1])
    wait_bytes(mid_all.at[peers_yc], yc_send.at[0])
    wait_bytes(db.at[peers_yc], yc_send.at[1])
    wait_bytes(fac.at[peers_yc], yc_send.at[2])
    for k in range(CHUNKS):
        wait_bytes(snd.at[others(k), pl.ds(0, ROWS)], pl_send.at[k])
    wait_bytes(rb.at[pl.ds(1, n_ep - 1), pl.ds(0, ROWS)], pl_send.at[CHUNKS])


def emit_kernel(mixed_ref, state_ref, mixed_hbm, state_hbm, sem):
    step = state_ref.shape[0] // 4
    copies = [pltpu.make_async_copy(mixed_ref, mixed_hbm, sem.at[0])]
    for i in range(4):
        rows = pl.ds(i * step, step)
        copies.append(
            pltpu.make_async_copy(state_ref.at[rows], state_hbm.at[rows], sem.at[1 + i])
        )
    for copy in copies:
        copy.start()
    for copy in copies:
        copy.wait()


def emit(mixed, state):
    vmem = pl.BlockSpec(memory_space=pltpu.VMEM)
    hbm = pl.BlockSpec(memory_space=pltpu.HBM)
    return pl.pallas_call(
        emit_kernel,
        name="emit",
        out_shape=(
            jax.ShapeDtypeStruct(mixed.shape, mixed.dtype),
            jax.ShapeDtypeStruct(state.shape, state.dtype),
        ),
        in_specs=[vmem, vmem],
        out_specs=(hbm, hbm),
        scratch_shapes=[pltpu.SemaphoreType.DMA((5,))],
        compiler_params=pltpu.CompilerParams(vmem_limit_bytes=16 << 20),
    )(mixed, state)


def layer(sizes, small, weights, pw, state, expert, dense):
    n_ep, n_x, n_z = sizes
    n_yc = n_ep // n_z
    tokens, width = small[2].shape
    key_dim, value_dim = state.shape[1:]
    eg, dg = expert[0], dense[0]
    quarter, units = width // n_x, dg.shape[1]
    all_units = n_z * units
    flat = n_ep * PAD
    vmem = pl.BlockSpec(memory_space=pltpu.VMEM)
    hbm = pl.BlockSpec(memory_space=pltpu.HBM)
    dma = pltpu.SemaphoreType.DMA
    operands = (*small, *weights, pw, state, *expert, *dense)
    return pl.pallas_call(
        functools.partial(layer_kernel, sizes),
        name="layer",
        out_shape=(
            jax.ShapeDtypeStruct((tokens, quarter), BF16),
            jax.ShapeDtypeStruct(state.shape, F32),
        ),
        in_specs=[hbm] * len(operands),
        out_specs=(vmem, vmem),
        scratch_shapes=[pltpu.VMEM(a.shape, a.dtype) for a in (*small, *weights, pw)]
        + [
            pltpu.VMEM((tokens, key_dim), F32),
            pltpu.VMEM((tokens, key_dim), F32),
            pltpu.VMEM((tokens, value_dim), F32),
            pltpu.VMEM((tokens, key_dim), F32),
            pltpu.VMEM((tokens, value_dim), F32),
            pltpu.VMEM((n_x, tokens, quarter), BF16),
            pltpu.VMEM((flat, tokens), BF16),
            pltpu.VMEM((flat, tokens), BF16),
            pltpu.VMEM((flat, tokens), BF16),
        ]
        + [pltpu.VMEM(a.shape, a.dtype) for a in expert]
        + [
            pltpu.VMEM((n_z, 2, quarter, units), BF16),
            pltpu.VMEM((n_z, units, quarter), BF16),
            pltpu.VMEM((n_x, tokens, quarter), BF16),
            pltpu.VMEM((n_x, tokens, quarter), BF16),
            pltpu.VMEM((n_ep, PAD, width), BF16),
            pltpu.VMEM((n_ep, PAD, width), BF16),
            pltpu.VMEM((n_yc, tokens, quarter), BF16),
            pltpu.VMEM((tokens, width), BF16),
            pltpu.VMEM((n_yc, 8, 128), F32),
            pltpu.VMEM((n_z, n_yc, tokens, 2 * units), BF16),
            pltpu.VMEM((n_z, n_x, n_yc // n_x, tokens, 2 * units), BF16),
            pltpu.VMEM((n_yc, tokens, all_units), BF16),
            pltpu.VMEM((n_yc, tokens, quarter), BF16),
            pltpu.VMEM((n_yc, tokens, quarter), BF16),
            pltpu.VMEM((CHUNKS, n_x, n_ep // CHUNKS, PAD, quarter), BF16),
            pltpu.VMEM((CHUNKS, n_x, n_ep // CHUNKS, PAD, quarter), BF16),
            pltpu.VMEM((n_ep, PAD, quarter), BF16),
            pltpu.VMEM((n_ep, PAD, quarter), BF16),
            dma((14,)),
            dma((tokens // 8,)),
            dma((6,)),
            dma((2,)),
            dma((n_z,)),
            dma((3,)),
            dma((3,)),
            dma((n_z,)),
            dma((n_z,)),
            dma((CHUNKS,)),
            dma((CHUNKS,)),
            dma((3,)),
            dma((3,)),
            dma((CHUNKS + 1,)),
            dma((CHUNKS + 1,)),
        ],
        compiler_params=pltpu.CompilerParams(
            collective_id=0, has_side_effects=True, vmem_limit_bytes=40 << 20
        ),
    )(*in_hbm(*operands))


def body(
    sizes,
    hidden_in,
    carried_state,
    input_gain,
    query_weight,
    key_weight,
    value_weight,
    outgate_weight,
    decay_weight,
    decay_shift,
    head_gain,
    output_weight,
    channel_gain,
    branch_gate,
    routes,
    route_weights,
    expert_gate,
    expert_up,
    expert_down,
    dense_gate,
    dense_up,
    dense_down,
):
    mixed, new_state = layer(
        sizes,
        (
            routes.T,
            route_weights.T,
            hidden_in,
            input_gain,
            decay_shift,
            head_gain,
            channel_gain,
            branch_gate,
        ),
        (query_weight, key_weight, value_weight, outgate_weight, decay_weight),
        output_weight,
        carried_state[:, 0],
        (expert_gate[0], expert_up[0], expert_down[0]),
        (dense_gate, dense_up, dense_down),
    )
    mixed, new_state = emit(mixed, new_state)
    return (mixed, new_state[:, None])


def solution(mesh):
    in_specs = (
        P("ep", None),
        P("ep", "tp", None, None),
        P(),
        P(None, "tp"),
        P(None, "tp"),
        P(None, "tp"),
        P(None, "tp"),
        P(None, "tp"),
        P("ep", "tp"),
        P("tp", None),
        P("tp", None),
        P(),
        P(),
        P("ep", None),
        P("ep", None),
        P("ep", None, "tp"),
        P("ep", None, "tp"),
        P("ep", "tp", None),
        P("tp", "ep"),
        P("tp", "ep"),
        P("ep", "tp"),
    )
    out_specs = (P("ep", "tp"), P("ep", "tp", None, None))
    n_ep = mesh.shape["ep"]
    sizes = (n_ep, mesh.shape["tp"], min(Z_SIZE, n_ep // 2))
    return jax.shard_map(
        functools.partial(body, sizes),
        mesh=mesh,
        in_specs=in_specs,
        out_specs=out_specs,
        check_vma=False,
    )
```

time: 169 us -> 59.3 us (0.35); the launches traced: 166 us -> 59.2 us
  Pallas kernels: 0 us -> 58.5 us
  waiting for transfers between devices: 51.5 us -> 0 us
  matrix products: 32.9 us -> 0 us
  starting transfers between devices: 26.2 us -> 0 us
  other arithmetic: 22.6 us -> 0 us
  local copies, waits for them, and re-layouts: 18.5 us -> 0 us
  between operations: 14.3 us -> 0.65 us
    pallas_call x0 -> x2, Pallas kernels: none -> 58.5 us  [the longest x1 55.8 us: layer(): pl.pallas_call(functools.partial(layer_kernel, sizes), name='layer', out_...]
    all_to_all x4 -> x0, waiting for transfers between devices: 39.2 us -> none  [the longest x1 23.4 us: body(): lax.all_to_all(outgoing, 'ep', split_axis=0, concat_axis=0, tiled=True)]
    dot_general x12 -> x0, matrix products: 32.9 us -> none  [the longest x11 29 us: matmul(): return jnp.dot(left, right, preferred_element_type=jnp.float32)]
    all_to_all x4 -> x0, starting transfers between devices: 26.1 us -> none  [the longest x1 10.3 us: body(): lax.all_to_all(outgoing, 'ep', split_axis=0, concat_axis=0, tiled=True)]
    psum x1 -> x0, waiting for transfers between devices: 12.3 us -> none  [unit_totals(): return lax.psum(paired.astype(jnp.bfloat16), 'tp').astype(jnp.float32)]
    reshape x7 -> x0, local copies, waits for them, and re-layouts: 8.42 us -> none  [the longest x1 2.19 us: body(): matmul(selector, send_rows).astype(jnp.bfloat16)]
    add x1 -> x0, other arithmetic: 7.31 us -> none  [body(): decay[..., None] * carried_state]
    reduce_sum x9 -> x0, other arithmetic: 5.81 us -> none  [the longest x3 1.32 us: rms_factor(): jnp.mean(values * values, axis=-1, keepdims=True) + EPSILON]
  transfers between devices with their start and end apart: 6 -> 0, of which waited for: 4 -> 0; matrix products, arithmetic and copies ran while one was open for 39% -> 0% of each run, Pallas kernels for 0% -> 0%
where the time goes in v3:
time: 59.3 us; the launch traced here: 59.2 us
  Pallas kernels  58.5 us (99%)
  between operations  0.65 us (1%)
    pallas_call x1, Pallas kernels, layer(): pl.pallas_call(functools.partial(layer_kernel, sizes), name='layer', out_...  55.8 us
    pallas_call x1, Pallas kernels, emit(): pl.pallas_call(emit_kernel, name='emit', out_shape=(jax.ShapeDtypeStruct(...  2.76 us

profile of v3, /device:TPU:1, one launch (start us, length us, event | category | flops | bytes accessed | tf_op | source)
XLA Modules:
  0.0 59.2 jit_solution(14438018714953486104)
XLA Ops:
  0.6 55.8 %layer.1 = (bf16[48,512]{1,0:T(8,128)(2,1)S(1)}, f32[48,128,256]{2,1,0:T(8,128)S(1)}) custom-call(s32[2,48]{1,0:T(2,128)} %bitcast.13, f32[2,48]{1,0:T(2,128)} %bitcast.14, bf16[48,2048]{1,0:T(8,128)(2,1)} %hid_hbm.1, bf16[2048]{0:T(1024)(128)(2,1)} %gain_hbm.1, f32[48,128]{1,0:T(8,128)} %shift_hbm.1, bf16[1,256]{1,0:T(2,128)(2,1)} %hgain_hbm.1, ...), custom_call_target="tpu_custom_call" | custom-call | tf_op jit(solution)/shard_map/layer/pallas_call | solution.py:542
  56.4 2.8 %emit.1 = (bf16[48,512]{1,0:T(8,128)(2,1)}, f32[48,128,256]{2,1,0:T(8,128)}) custom-call(bf16[48,512]{1,0:T(8,128)(2,1)S(1)} %get-tuple-element.6.mixed_ref, f32[48,128,256]{2,1,0:T(8,128)S(1)} %get-tuple-element.7.state_ref), custom_call_target="tpu_custom_call" | custom-call | tf_op jit(solution)/shard_map/emit/pallas_call | solution.py:515

commit v4 on v3

--- a/solution.py
+++ b/solution.py
@@ -17,6 +17,7 @@
 CHUNKS = 4
 EARLY = 2
 FLIGHT = 2
+GROUP = 16
 Z_SIZE = 4
 F32 = jnp.float32
 BF16 = jnp.bfloat16
@@ -86,6 +87,7 @@
     v_s,
     d_s,
     ro_s,
+    og_s,
     part,
     sel_ref,
     comb_hi_ref,
@@ -218,7 +220,7 @@
         copy.start()
     for g in range(groups):
         state_in(g).start()
-    for copy in w_copies[4:] + e_copies:
+    for copy in w_copies[4:]:
         copy.start()
 
     for copy in s_copies[:2]:
@@ -252,14 +254,6 @@
     comb_hi_ref[...] = comb_hi
     comb_lo_ref[...] = (comb - comb_hi.astype(F32)).astype(BF16)
 
-    for copy in d_copies:
-        copy.wait()
-    pl.semaphore_wait(barrier, n_x - 1 + n_ep - 1)
-    near_first = [1, n_z - 1] + list(range(2, n_z - 1))
-    for i in near_first:
-        b = n_z - i
-        remote(wgu.at[0], wgu.at[b], wz_send.at[0], wz_recv.at[b], z_peer(i)).start()
-
     for copy in s_copies[2:]:
         copy.wait()
     hid = hid_s[...].astype(F32)
@@ -269,53 +263,97 @@
     log_sig = jnp.minimum(pre, 0.0) - jnp.log1p(jnp.exp(-jnp.abs(pre)))
     d_s[...] = jnp.exp(log_sig / TAU_DECAY + shift_s[...])
     w_copies[1].wait()
-    q_s[...] = dot(normed, qw[...]).astype(BF16).astype(F32) * key_dim ** (-0.5)
+    q_s[...] = dot(normed, qw[...]).astype(BF16).astype(F32)
     w_copies[2].wait()
     k_s[...] = dot(normed, kw[...]).astype(BF16).astype(F32)
     w_copies[3].wait()
     v_s[...] = dot(normed, vw[...]).astype(BF16).astype(F32)
 
+    for copy in d_copies:
+        copy.wait()
+    pl.semaphore_wait(barrier, n_x - 1 + n_ep - 1)
+    near_first = [1, n_z - 1] + list(range(2, n_z - 1))
+    for i in near_first:
+        b = n_z - i
+        remote(wgu.at[0], wgu.at[b], wz_send.at[0], wz_recv.at[b], z_peer(i)).start()
+
+    span = GROUP * key_dim
+    at_block = lax.broadcasted_iota(jnp.int32, (GROUP, span), 1) // key_dim
+    on_block = at_block == lax.broadcasted_iota(jnp.int32, (GROUP, span), 0)
+
+    def spread(rows):
+        return jnp.where(on_block, jnp.concatenate([rows] * GROUP, axis=1), 0.0).astype(BF16)
+
     def group(g, carry):
-        state_in(g).wait()
-        rows = pl.ds(pl.multiple_of(g * 8, 8), 8)
-        d_t, k_t, q_t = d_s[rows, :].T, k_s[rows, :].T, q_s[rows, :].T
-        v_8 = v_s[rows, :]
-        outs = []
-        for j in range(8):
-            b = g * 8 + j
-            new = d_t[:, j : j + 1] * state_out[b] + k_t[:, j : j + 1] * v_8[j : j + 1, :]
+        for part_of in range(GROUP // 8):
+            state_in(g * (GROUP // 8) + part_of).wait()
+        rows = pl.ds(pl.multiple_of(g * GROUP, GROUP), GROUP)
+        d_t = d_s[rows, :].T
+        outer = turned_dot(spread(k_s[rows, :]), v_s[rows, :].astype(BF16))
+        news = []
+        for j in range(GROUP):
+            b = g * GROUP + j
+            added = outer[j * key_dim : (j + 1) * key_dim, :]
+            new = d_t[:, j : j + 1] * state_out[b] + added
             state_out[b] = new
-            outs.append(jnp.sum(q_t[:, j : j + 1] * new, axis=0, keepdims=True))
-        ro_s[rows, :] = jnp.concatenate(outs, axis=0)
+            news.append(new.astype(BF16))
+        ro_s[rows, :] = dot(spread(q_s[rows, :]), jnp.concatenate(news, axis=0))
         return carry
 
-    lax.fori_loop(0, groups, group, 0)
+    cut = tokens - GROUP
+    parts = (slice(0, cut), slice(cut, tokens))
+
+    def rows_of(p):
+        return pl.ds(parts[p].start, parts[p].stop - parts[p].start)
+
+    def send_heads(p):
+        readout = ro_s[parts[p], :] * key_dim ** (-0.5)
+        gated = readout * rms_factor(readout) * hgain_s[...].astype(F32) * og_s[parts[p], :]
+        gated = gated.astype(BF16)
+        for i in range(1, n_x):
+            part[i, parts[p]] = dot(gated, pw[:, lanes(i)]).astype(BF16)
+            remote(
+                part.at[i, rows_of(p)],
+                rs1.at[i, rows_of(p)],
+                x_send.at[p],
+                x_recv.at[p],
+                x_peer(i),
+            ).start()
+        return dot(gated, pw[:, lanes(0)]).astype(BF16).astype(F32)
+
+    def send_middle(p, total):
+        wait_bytes(rs1.at[peers_x, rows_of(p)], x_recv.at[p])
+        for i in range(1, n_x):
+            total = total + rs1[i, parts[p]].astype(F32)
+        middle_q = (hid_s[parts[p], lanes(0)].astype(F32) + total).astype(BF16)
+        mid[pl.ds(x, 1), parts[p]] = middle_q[None]
+        mid_all[pl.ds(yc, 1), parts[p]] = middle_q[None]
+        for i in range(1, n_x):
+            mine = mid.at[x, rows_of(p)]
+            remote(mine, mine, x_send.at[2 + p], x_recv.at[2 + p], x_peer(i)).start()
+        for i in range(1, n_yc):
+            mine = mid_all.at[yc, rows_of(p)]
+            remote(mine, mine, yc_send.at[p], yc_recv.at[p], yc_peer(i)).start()
+
+    lax.fori_loop(0, cut // GROUP, group, 0)
 
     w_copies[4].wait()
-    outgate = dot(normed, ow[...]).astype(BF16).astype(F32)
-    readout = ro_s[...]
-    gated = readout * rms_factor(readout) * hgain_s[...].astype(F32) * silu(outgate)
-    gated = gated.astype(BF16)
+    og_s[...] = silu(dot(normed, ow[...]).astype(BF16).astype(F32))
     w_copies[5].wait()
-
-    for i in range(1, n_x):
-        part[i] = dot(gated, pw[:, lanes(i)]).astype(BF16)
-        remote(part.at[i], rs1.at[i], x_send.at[0], x_recv.at[0], x_peer(i)).start()
-    total = dot(gated, pw[:, lanes(0)]).astype(BF16).astype(F32)
-
-    wait_bytes(rs1.at[peers_x], x_recv.at[0])
-    for i in range(1, n_x):
-        total = total + rs1[i].astype(F32)
-    middle_q = (hid_s[:, lanes(0)].astype(F32) + total).astype(BF16)
-    mid[pl.ds(x, 1)] = middle_q[None]
-    mid_all[pl.ds(yc, 1)] = middle_q[None]
-
-    for i in range(1, n_x):
-        remote(mid.at[x], mid.at[x], x_send.at[1], x_recv.at[1], x_peer(i)).start()
-    for i in range(1, n_yc):
-        remote(mid_all.at[yc], mid_all.at[yc], yc_send.at[0], yc_recv.at[0], yc_peer(i)).start()
-
-    wait_bytes(mid.at[peers_x], x_recv.at[1])
+    total_1 = send_heads(0)
+
+    lax.fori_loop(cut // GROUP, tokens // GROUP, group, 0)
+
+    total_2 = send_heads(1)
+    for copy in e_copies:
+        copy.start()
+
+    send_middle(0, total_1)
+
+    send_middle(1, total_2)
+
+    for p in range(2):
+        wait_bytes(mid.at[peers_x, rows_of(p)], x_recv.at[2 + p])
 
     squares = sum(
         jnp.sum(mid[i].astype(F32) * mid[i].astype(F32), axis=-1, keepdims=True) for i in range(n_x)
@@ -356,9 +394,10 @@
     factor_rows = jnp.broadcast_to(factor, (tokens, 128)).T[0:8, :]
     fac[pl.ds(yc, 1), :, 0:tokens] = factor_rows[None]
     for i in range(1, n_yc):
-        remote(fac.at[yc], fac.at[yc], yc_send.at[2], yc_recv.at[2], yc_peer(i)).start()
-
-    wait_bytes(mid_all.at[peers_yc], yc_recv.at[0])
+        remote(fac.at[yc], fac.at[yc], yc_send.at[3], yc_recv.at[3], yc_peer(i)).start()
+
+    for p in range(2):
+        wait_bytes(mid_all.at[peers_yc, rows_of(p)], yc_recv.at[p])
 
     per_x = n_yc // n_x
     gain_q = cgain_s[lanes(0)][None, :].astype(F32)
@@ -368,9 +407,7 @@
     def group_of(i):
         return pl.ds(lax.rem(x + i, n_x) * per_x, per_x)
 
-    for b in [0] + near_first:
-        if b:
-            wait_bytes(wgu.at[b], wz_recv.at[b])
+    def gate_up(b):
         paired = dot(rows_in, jnp.concatenate([wgu[b, 0], wgu[b, 1]], axis=1))
         pr[b] = paired.astype(BF16).reshape(n_yc, tokens, 2 * units)
         for i in range(1, n_x):
@@ -378,6 +415,12 @@
                 pr.at[b, group_of(i)], rs2.at[b, i], r_send.at[b], r_recv.at[b], x_peer(i)
             ).start()
 
+    gate_up(0)
+
+    for b in near_first:
+        wait_bytes(wgu.at[b], wz_recv.at[b])
+        gate_up(b)
+
     for copy in e_copies:
         copy.wait()
     flat = per_chunk * PAD
@@ -386,6 +429,10 @@
         wait_bytes(rcv.at[others(k), pl.ds(0, ROWS)], pl_recv.at[k])
         if k + FLIGHT < CHUNKS:
             dispatch(k + FLIGHT)
+            if k + FLIGHT == CHUNKS - 1:
+                for i in near_first:
+                    b = n_z - i
+                    remote(wd.at[0], wd.at[b], wz_send.at[1], wz_recv.at[0], z_peer(i)).start()
         rows = rcv[chunk(k)].reshape(flat, width)
         hidden = (silu(dot(rows, eg[...])) * dot(rows, eu[...])).astype(BF16)
         for i in list(range(1, n_x)) + [0]:
@@ -403,7 +450,7 @@
     for k in range(EARLY):
         run_expert(k)
 
-    wait_bytes(fac.at[peers_yc], yc_recv.at[2])
+    wait_bytes(fac.at[peers_yc], yc_recv.at[3])
     factors = jnp.concatenate(
         [fac[pl.ds(x * per_x + b, 1)][0].T[0:tokens, 0:1] for b in range(per_x)], axis=0
     )
@@ -420,12 +467,10 @@
         remote(
             hid_all.at[group_of(0)],
             hid_all.at[group_of(0)],
-            x_send.at[2],
-            x_recv.at[2],
+            x_send.at[4],
+            x_recv.at[4],
             x_peer(i),
         ).start()
-    for i in near_first:
-        remote(wd.at[0], wd.at[n_z - i], wz_send.at[1], wz_recv.at[0], z_peer(i)).start()
 
     for k in range(EARLY, CHUNKS):
         run_expert(k)
@@ -451,7 +496,7 @@
     for k in range(EARLY):
         go_home(k)
 
-    wait_bytes(hid_all.at[pl.ds(0, n_yc - per_x)], x_recv.at[2])
+    wait_bytes(hid_all.at[pl.ds(0, n_yc - per_x)], x_recv.at[4])
 
     wait_bytes(wd.at[peers_z], wz_recv.at[0])
     dense_part = dot(
@@ -460,14 +505,14 @@
     db[...] = dense_part.reshape(n_yc, tokens, quarter).astype(BF16)
     for i in range(1, n_yc):
         remote(
-            db.at[lax.rem(yc + i, n_yc)], dr.at[i], yc_send.at[1], yc_recv.at[1], yc_peer(i)
+            db.at[lax.rem(yc + i, n_yc)], dr.at[i], yc_send.at[2], yc_recv.at[2], yc_peer(i)
         ).start()
 
     for k in range(EARLY, CHUNKS):
         go_home(k)
 
     dense = db[pl.ds(yc, 1)][0].astype(F32)
-    wait_bytes(dr.at[peers_yc], yc_recv.at[1])
+    wait_bytes(dr.at[peers_yc], yc_recv.at[2])
     for i in range(1, n_yc):
         dense = dense + dr[i].astype(F32)
 
@@ -478,18 +523,19 @@
     middle_own = mid[pl.ds(x, 1)][0].astype(F32)
     out_ref[...] = (middle_own + branch * dense + routed).astype(BF16)
 
-    wait_bytes(part.at[peers_x], x_send.at[0])
-    wait_bytes(mid.at[peers_x], x_send.at[1])
-    wait_bytes(hid_all.at[pl.ds(0, n_yc - per_x)], x_send.at[2])
+    for p in range(2):
+        wait_bytes(part.at[peers_x, rows_of(p)], x_send.at[p])
+        wait_bytes(mid.at[peers_x, rows_of(p)], x_send.at[2 + p])
+        wait_bytes(mid_all.at[peers_yc, rows_of(p)], yc_send.at[p])
+    wait_bytes(hid_all.at[pl.ds(0, n_yc - per_x)], x_send.at[4])
     for b in range(n_z):
         wait_bytes(rs2.at[b, peers_x], r_send.at[b])
     for k in range(CHUNKS):
         wait_bytes(yb.at[k, peers_x, :, pl.ds(0, ROWS)], y_send.at[k])
     wait_bytes(wgu.at[peers_z], wz_send.at[0])
     wait_bytes(wd.at[peers_z], wz_send.at[1])
-    wait_bytes(mid_all.at[peers_yc], yc_send.at[0])
-    wait_bytes(db.at[peers_yc], yc_send.at[1])
-    wait_bytes(fac.at[peers_yc], yc_send.at[2])
+    wait_bytes(db.at[peers_yc], yc_send.at[2])
+    wait_bytes(fac.at[peers_yc], yc_send.at[3])
     for k in range(CHUNKS):
         wait_bytes(snd.at[others(k), pl.ds(0, ROWS)], pl_send.at[k])
     wait_bytes(rb.at[pl.ds(1, n_ep - 1), pl.ds(0, ROWS)], pl_send.at[CHUNKS])
@@ -554,6 +600,7 @@
             pltpu.VMEM((tokens, key_dim), F32),
             pltpu.VMEM((tokens, value_dim), F32),
             pltpu.VMEM((tokens, key_dim), F32),
+            pltpu.VMEM((tokens, value_dim), F32),
             pltpu.VMEM((tokens, value_dim), F32),
             pltpu.VMEM((n_x, tokens, quarter), BF16),
             pltpu.VMEM((flat, tokens), BF16),
@@ -585,14 +632,14 @@
             dma((6,)),
             dma((2,)),
             dma((n_z,)),
-            dma((3,)),
-            dma((3,)),
+            dma((5,)),
+            dma((5,)),
             dma((n_z,)),
             dma((n_z,)),
             dma((CHUNKS,)),
             dma((CHUNKS,)),
-            dma((3,)),
-            dma((3,)),
+            dma((4,)),
+            dma((4,)),
             dma((CHUNKS + 1,)),
             dma((CHUNKS + 1,)),
         ],

time: 59.3 us -> 54.7 us (0.922)
  Pallas kernels: 58.5 us -> 53.9 us
    pallas_call x1, Pallas kernels: 55.8 us -> 51.2 us  [layer(): pl.pallas_call(functools.partial(layer_kernel, sizes), name='layer', out_...]
where the time goes in v4:
time: 54.7 us; the launch traced here: 54.6 us
  Pallas kernels  53.9 us (99%)
  between operations  0.65 us (1%)
    pallas_call x1, Pallas kernels, layer(): pl.pallas_call(functools.partial(layer_kernel, sizes), name='layer', out_...  51.2 us
    pallas_call x1, Pallas kernels, emit(): pl.pallas_call(emit_kernel, name='emit', out_shape=(jax.ShapeDtypeStruct(...  2.76 us

profile of v4, /device:TPU:1, one launch (start us, length us, event | category | flops | bytes accessed | tf_op | source)
XLA Modules:
  0.0 54.6 jit_solution(12855995251510785914)
XLA Ops:
  0.6 51.2 %layer.1 = (bf16[48,512]{1,0:T(8,128)(2,1)S(1)}, f32[48,128,256]{2,1,0:T(8,128)S(1)}) custom-call(s32[2,48]{1,0:T(2,128)} %bitcast.13, f32[2,48]{1,0:T(2,128)} %bitcast.14, bf16[48,2048]{1,0:T(8,128)(2,1)} %hid_hbm.1, bf16[2048]{0:T(1024)(128)(2,1)} %gain_hbm.1, f32[48,128]{1,0:T(8,128)} %shift_hbm.1, bf16[1,256]{1,0:T(2,128)(2,1)} %hgain_hbm.1, ...), custom_call_target="tpu_custom_call" | custom-call | tf_op jit(solution)/shard_map/layer/pallas_call | solution.py:588
  51.8 2.8 %emit.1 = (bf16[48,512]{1,0:T(8,128)(2,1)}, f32[48,128,256]{2,1,0:T(8,128)}) custom-call(bf16[48,512]{1,0:T(8,128)(2,1)S(1)} %get-tuple-element.6.mixed_ref, f32[48,128,256]{2,1,0:T(8,128)S(1)} %get-tuple-element.7.state_ref), custom_call_target="tpu_custom_call" | custom-call | tf_op jit(solution)/shard_map/emit/pallas_call | solution.py:561

commit v5 on v4

--- a/solution.py
+++ b/solution.py
@@ -269,14 +269,6 @@
     w_copies[3].wait()
     v_s[...] = dot(normed, vw[...]).astype(BF16).astype(F32)
 
-    for copy in d_copies:
-        copy.wait()
-    pl.semaphore_wait(barrier, n_x - 1 + n_ep - 1)
-    near_first = [1, n_z - 1] + list(range(2, n_z - 1))
-    for i in near_first:
-        b = n_z - i
-        remote(wgu.at[0], wgu.at[b], wz_send.at[0], wz_recv.at[b], z_peer(i)).start()
-
     span = GROUP * key_dim
     at_block = lax.broadcasted_iota(jnp.int32, (GROUP, span), 1) // key_dim
     on_block = at_block == lax.broadcasted_iota(jnp.int32, (GROUP, span), 0)
@@ -336,6 +328,14 @@
             remote(mine, mine, yc_send.at[p], yc_recv.at[p], yc_peer(i)).start()
 
     lax.fori_loop(0, cut // GROUP, group, 0)
+
+    for copy in d_copies:
+        copy.wait()
+    pl.semaphore_wait(barrier, n_x - 1 + n_ep - 1)
+    near_first = [1, n_z - 1] + list(range(2, n_z - 1))
+    for i in near_first:
+        b = n_z - i
+        remote(wgu.at[0], wgu.at[b], wz_send.at[0], wz_recv.at[b], z_peer(i)).start()
 
     w_copies[4].wait()
     og_s[...] = silu(dot(normed, ow[...]).astype(BF16).astype(F32))

time: 54.7 us -> 53.5 us (0.978)
  Pallas kernels: 53.9 us -> 52.8 us
    pallas_call x1, Pallas kernels: 51.2 us -> 50 us  [layer(): pl.pallas_call(functools.partial(layer_kernel, sizes), name='layer', out_...]
where the time goes in v5:
time: 53.5 us; the launch traced here: 53.4 us
  Pallas kernels  52.8 us (99%)
  between operations  0.65 us (1%)
    pallas_call x1, Pallas kernels, layer(): pl.pallas_call(functools.partial(layer_kernel, sizes), name='layer', out_...  50 us
    pallas_call x1, Pallas kernels, emit(): pl.pallas_call(emit_kernel, name='emit', out_shape=(jax.ShapeDtypeStruct(...  2.76 us

profile of v5, /device:TPU:1, one launch (start us, length us, event | category | flops | bytes accessed | tf_op | source)
XLA Modules:
  0.0 53.4 jit_solution(1420429237628139840)
XLA Ops:
  0.6 50.0 %layer.1 = (bf16[48,512]{1,0:T(8,128)(2,1)S(1)}, f32[48,128,256]{2,1,0:T(8,128)S(1)}) custom-call(s32[2,48]{1,0:T(2,128)} %bitcast.13, f32[2,48]{1,0:T(2,128)} %bitcast.14, bf16[48,2048]{1,0:T(8,128)(2,1)} %hid_hbm.1, bf16[2048]{0:T(1024)(128)(2,1)} %gain_hbm.1, f32[48,128]{1,0:T(8,128)} %shift_hbm.1, bf16[1,256]{1,0:T(2,128)(2,1)} %hgain_hbm.1, ...), custom_call_target="tpu_custom_call" | custom-call | tf_op jit(solution)/shard_map/layer/pallas_call | solution.py:588
  50.6 2.8 %emit.1 = (bf16[48,512]{1,0:T(8,128)(2,1)}, f32[48,128,256]{2,1,0:T(8,128)}) custom-call(bf16[48,512]{1,0:T(8,128)(2,1)S(1)} %get-tuple-element.6.mixed_ref, f32[48,128,256]{2,1,0:T(8,128)S(1)} %get-tuple-element.7.state_ref), custom_call_target="tpu_custom_call" | custom-call | tf_op jit(solution)/shard_map/emit/pallas_call | solution.py:561
